TPU v7x, 256 devices: a whole 4x4x8 slice. The times are simulated.
256 devices in a mesh: kv: 32 (over z, x), tp: 8 (over y, core).
Axes of the slice: x: 4, y: 4, z: 8, core: 2. Of those that a mesh axis runs over, the one named last changes fastest.
Arguments:
- tokens: bfloat16 [32768, 2048], P('kv'), may hold values from -72 to 72
- query_weight: bfloat16 [2048, 2048], P(None, 'tp'), may hold values from -0.125 to 0.125
- key_projection_matrix: bfloat16 [2048, 1024], P(None, 'tp'), may hold values from -0.125 to 0.125
- value_projection_matrix: bfloat16 [2048, 1024], P(None, 'tp'), may hold values from -0.125 to 0.125
- out_weight: bfloat16 [2048, 2048], P('tp'), may hold values from -1.5 to 1.5
- chosen: int32 [256, 12], P('kv'), may hold values from -1 to 1023, as said below
Outputs:
- layer_out: bfloat16 [32768, 2048], P(('kv', 'tp'))
Inputs may be any that keep to these rules, and one draw needn't show every extreme that they name: `chosen`: positions are grouped in consecutive groups of 1024. The blocks named in one row lie in distinct groups, all earlier than the group of the row's query block; a query block in group g has exactly min(12, g) entries that are not -1, first in its row, and the rest are -1. So the query blocks of one group name at most 8 blocks of any one other group, and in every draw some group's query blocks all name blocks of one same earlier group.
All inputs are finite; a program needn't handle non-finite values.
Results may differ from a plain program's by a relative error of at most 0.014.
The roundings to bfloat16 on the way count: a program that leaves them out, or rounds other values in their place, can miss the bound.
Values may be sent and summed in bfloat16 or wider, within the bound.
A program may use at most 64 MiB of HBM per device.

v0:
```python
import jax
import jax.numpy as jnp
from jax import lax
from jax.sharding import PartitionSpec as P

HEAD_SIZE = 128
QUERY_BLOCK_SPAN = 128
KEY_BLOCK_SPAN = 32
NFAR = 12


def joined_along(blocks, dim):
    dims = list(blocks.shape[1:])
    dims[dim] *= blocks.shape[0]
    return jnp.moveaxis(blocks, 0, dim).reshape(dims)


def from_everyone(x, axis):
    size = lax.axis_size(axis)
    return lax.all_to_all(jnp.broadcast_to(x[None], (size, *x.shape)), axis, 0, 0, tiled=True)


def gather_directly(x, axis, dim):
    return joined_along(from_everyone(x, axis), dim)


def shards(
    tokens, query_weight, key_projection_matrix, value_projection_matrix, out_weight, chosen
):
    tok_rows = tokens.shape[0]
    kv_width = key_projection_matrix.shape[1]
    kv_heads = kv_width // HEAD_SIZE
    q_heads = query_weight.shape[1] // HEAD_SIZE
    grouped_head_index = q_heads // kv_heads
    query_blocks = tok_rows // QUERY_BLOCK_SPAN
    blocked_keys = tok_rows // KEY_BLOCK_SPAN
    queries = jnp.dot(tokens, query_weight, preferred_element_type=jnp.float32).astype(jnp.bfloat16)
    key_vectors = jnp.dot(tokens, key_projection_matrix, preferred_element_type=jnp.float32).astype(
        jnp.bfloat16
    )
    value_vectors = jnp.dot(
        tokens, value_projection_matrix, preferred_element_type=jnp.float32
    ).astype(jnp.bfloat16)
    my_index = lax.axis_index("kv")
    key_rows = key_vectors.reshape(blocked_keys, KEY_BLOCK_SPAN, kv_width)
    value_rows = value_vectors.reshape(blocked_keys, KEY_BLOCK_SPAN, kv_width)
    all_lists = gather_directly(chosen, "kv", 0)
    peer_count = all_lists.shape[0] // query_blocks
    asked_ids = all_lists.reshape(peer_count, query_blocks, NFAR)
    is_mine = (asked_ids >= 0) & (asked_ids // blocked_keys == my_index)
    wanted = jnp.sum(jnp.where(is_mine, asked_ids - my_index * blocked_keys, 0), axis=2)
    received = (
        lax.all_to_all(key_rows[wanted], "kv", split_axis=0, concat_axis=0, tiled=True),
        lax.all_to_all(value_rows[wanted], "kv", split_axis=0, concat_axis=0, tiled=True),
    )
    owners = jnp.where(chosen >= 0, chosen // blocked_keys, 0)
    block_slot = jnp.arange(query_blocks, dtype=jnp.int32)[:, None]
    far_keys = received[0][owners, block_slot]
    far_values = received[1][owners, block_slot]
    listed_keys = QUERY_BLOCK_SPAN + NFAR * KEY_BLOCK_SPAN
    row_offset = my_index * tok_rows
    query_pos = row_offset + jnp.arange(tok_rows, dtype=jnp.int32).reshape(
        query_blocks, QUERY_BLOCK_SPAN
    )
    far_pos = (
        jnp.maximum(chosen, 0)[:, :, None] * KEY_BLOCK_SPAN
        + jnp.arange(KEY_BLOCK_SPAN, dtype=jnp.int32)
    ).reshape(query_blocks, NFAR * KEY_BLOCK_SPAN)
    far_ok = jnp.broadcast_to(
        (chosen >= 0)[:, :, None], (query_blocks, NFAR, KEY_BLOCK_SPAN)
    ).reshape(query_blocks, NFAR * KEY_BLOCK_SPAN)
    key_pos = jnp.concatenate([query_pos, far_pos], axis=1)
    key_ok = jnp.concatenate(
        [jnp.ones((query_blocks, QUERY_BLOCK_SPAN), dtype=bool), far_ok], axis=1
    )
    allowed = key_ok[:, None, :] & (key_pos[:, None, :] <= query_pos[:, :, None])
    all_keys = jnp.concatenate(
        [
            key_vectors.reshape(query_blocks, QUERY_BLOCK_SPAN, kv_width),
            far_keys.reshape(query_blocks, NFAR * KEY_BLOCK_SPAN, kv_width),
        ],
        axis=1,
    )
    all_values = jnp.concatenate(
        [
            value_vectors.reshape(query_blocks, QUERY_BLOCK_SPAN, kv_width),
            far_values.reshape(query_blocks, NFAR * KEY_BLOCK_SPAN, kv_width),
        ],
        axis=1,
    )
    grouped = queries.reshape(
        query_blocks, QUERY_BLOCK_SPAN, kv_heads, grouped_head_index, HEAD_SIZE
    )
    scores = jnp.einsum(
        "bqgrd,bkgd->bgrqk",
        grouped,
        all_keys.reshape(query_blocks, listed_keys, kv_heads, HEAD_SIZE),
        preferred_element_type=jnp.float32,
    ) * HEAD_SIZE ** (-0.5)
    scores = jnp.where(allowed[:, None, None], scores, -jnp.inf)
    row_max = jnp.max(scores, axis=-1, keepdims=True)
    exp_scores = jnp.exp(scores - row_max)
    row_sum = jnp.sum(exp_scores, axis=-1, keepdims=True)
    weights = (exp_scores / row_sum).astype(jnp.bfloat16)
    mixed = jnp.einsum(
        "bgrqk,bkgd->bqgrd",
        weights,
        all_values.reshape(query_blocks, listed_keys, kv_heads, HEAD_SIZE),
        preferred_element_type=jnp.float32,
    )
    mixed = mixed.astype(jnp.bfloat16).reshape(tok_rows, q_heads * HEAD_SIZE)
    return lax.psum_scatter(
        jnp.dot(mixed, out_weight, preferred_element_type=jnp.float32).astype(jnp.bfloat16),
        "tp",
        scatter_dimension=0,
        tiled=True,
    )


def solution(mesh):
    return jax.shard_map(
        shards,
        mesh=mesh,
        in_specs=(
            P("kv", None),
            P(None, "tp"),
            P(None, "tp"),
            P(None, "tp"),
            P("tp", None),
            P("kv", None),
        ),
        out_specs=P(("kv", "tp"), None),
        check_vma=False,
    )
```

profile of v0, /device:TPU:6, one launch (start us, length us, event | category | flops | bytes accessed | tf_op | source)
XLA Modules:
  0.0 195.8 jit_solution(3449374113824474936)
XLA Ops:
  6.5 1.4 broadcast_in_dim.20
  8.0 11.6 %all-to-all-start = ((s32[32,8,12]{2,1,0:T(8,128)}), s32[32,8,12]{2,1,0:T(8,128)S(1)}, u32[]{:S(2)}, u32[]{:S(2)}) async-start(s32[32,8,12]{2,1,0:T(8,128)} %broadcast_in_dim.20), calls=%async_computation | async-start | bytes 262144 | tf_op jit(solution)/shard_map/all_to_all | solution.py:20
  19.5 3.5 %convolution_convert_fusion.3 = bf16[1024,128]{1,0:T(8,128)(2,1)S(1)} fusion(bf16[1024,2048]{1,0:T(8,128)(2,1)} %param.6, bf16[2048,128]{1,0:T(8,128)(2,1)} %param.9), kind=kOutput, calls=%fused_computation.18 | convolution fusion | flops 537001984 | bytes 4980736 | tf_op jit(solution)/shard_map/dot_general | solution.py:41
  23.1 5.4 %all-to-all-done = s32[32,8,12]{2,1,0:T(8,128)S(1)} async-done(((s32[32,8,12]{2,1,0:T(8,128)}), s32[32,8,12]{2,1,0:T(8,128)S(1)}, u32[]{:S(2)}, u32[]{:S(2)}) %all-to-all-start) | async-done | bytes 12320 | tf_op jit(solution)/shard_map/all_to_all | solution.py:20
  28.5 0.6 select_reduce_fusion
  29.4 2.2 %gather_fusion = bf16[256,32,128]{2,1,0:T(8,128)(2,1)} fusion(bf16[32,32,128]{2,1,0:T(8,128)(2,1)S(1)} %bitcast.72, s32[1024]{0:T(1024)S(1)} %pad_clamp_fusion), kind=kCustom, calls=%fused_computation | custom fusion | bytes 4195328 | tf_op jit(solution)/shard_map/gather | solution.py:54
  31.5 6.1 %all-to-all-start.1 = ((bf16[32,8,32,128]{3,2,1,0:T(8,128)(2,1)}), bf16[32,8,32,128]{3,2,1,0:T(8,128)(2,1)}, u32[]{:S(2)}, u32[]{:S(2)}) async-start(bf16[32,8,32,128]{3,2,1,0:T(8,128)(2,1)} %bitcast.3), calls=%async_computation.1 | async-start | bytes 4194304 | tf_op jit(solution)/shard_map/all_to_all | solution.py:54
  37.7 3.4 %convolution_convert_fusion.2 = bf16[1024,128]{1,0:T(8,128)(2,1)S(1)} fusion(bf16[1024,2048]{1,0:T(8,128)(2,1)} %param.6, bf16[2048,128]{1,0:T(8,128)(2,1)S(1)} %copy-done.4), kind=kOutput, calls=%fused_computation.17 | convolution fusion | flops 537001984 | bytes 4980736 | tf_op jit(solution)/shard_map/dot_general | solution.py:38
  41.1 2.2 %gather_fusion.2 = bf16[256,32,128]{2,1,0:T(8,128)(2,1)} fusion(bf16[32,32,128]{2,1,0:T(8,128)(2,1)S(1)} %bitcast.74, s32[1024]{0:T(1024)S(1)} %pad_clamp_fusion), kind=kCustom, calls=%fused_computation.2 | custom fusion | bytes 4195328 | tf_op jit(solution)/shard_map/gather | solution.py:53
  43.3 43.9 %all-to-all-done.1 = bf16[32,8,32,128]{3,2,1,0:T(8,128)(2,1)} async-done(((bf16[32,8,32,128]{3,2,1,0:T(8,128)(2,1)}), bf16[32,8,32,128]{3,2,1,0:T(8,128)(2,1)}, u32[]{:S(2)}, u32[]{:S(2)}) %all-to-all-start.1) | async-done | bytes 2097184 | tf_op jit(solution)/shard_map/all_to_all | solution.py:54
  87.2 5.6 %all-to-all-start.2 = ((bf16[32,8,32,128]{3,2,1,0:T(8,128)(2,1)}), bf16[32,8,32,128]{3,2,1,0:T(8,128)(2,1)}, u32[]{:S(2)}, u32[]{:S(2)}) async-start(bf16[32,8,32,128]{3,2,1,0:T(8,128)(2,1)} %bitcast.76), calls=%async_computation.2 | async-start | bytes 4194304 | tf_op jit(solution)/shard_map/all_to_all | solution.py:53
  93.6 0.9 copy.32
  94.5 3.7 %convolution_convert_fusion.1 = bf16[1024,256]{1,0:T(8,128)(2,1)S(1)} fusion(bf16[1024,2048]{1,0:T(8,128)(2,1)} %param.6, bf16[2048,256]{1,0:T(8,128)(2,1)} %param.7), kind=kOutput, calls=%fused_computation.15 | convolution fusion | flops 1074003968 | bytes 5767168 | tf_op jit(solution)/shard_map/dot_general | solution.py:37
  98.4 1.4 compare_and_fusion
  99.9 2.7 %gather_fusion.1 = bf16[96,32,128]{2,1,0:T(8,128)(2,1)S(1)} fusion(bf16[32,8,32,128]{3,2,1,0:T(8,128)(2,1)} %all-to-all-done.1, s32[96]{0:T(128)S(1)} %reshape.118), kind=kCustom, calls=%fused_computation.1 | custom fusion | bytes 1573632 | tf_op jit(solution)/shard_map/gather | solution.py:59
  102.6 1.2 copy.33
  103.8 37.1 %all-to-all-done.2 = bf16[32,8,32,128]{3,2,1,0:T(8,128)(2,1)} async-done(((bf16[32,8,32,128]{3,2,1,0:T(8,128)(2,1)}), bf16[32,8,32,128]{3,2,1,0:T(8,128)(2,1)}, u32[]{:S(2)}, u32[]{:S(2)}) %all-to-all-start.2) | async-done | bytes 2097184 | tf_op jit(solution)/shard_map/all_to_all | solution.py:53
  141.0 2.7 %gather_fusion.3 = bf16[96,32,128]{2,1,0:T(8,128)(2,1)S(1)} fusion(bf16[32,8,32,128]{3,2,1,0:T(8,128)(2,1)} %all-to-all-done.2, s32[96]{0:T(128)S(1)} %reshape.118), kind=kCustom, calls=%fused_computation.3 | custom fusion | bytes 1573632 | tf_op jit(solution)/shard_map/gather | solution.py:58
  143.7 0.8 fusion.1
  144.5 1.0 fusion
  145.7 1.3 fusion.8
  147.0 0.3 copy.36
  147.4 3.2 %convolution_convert_fusion = bf16[1024,2048]{1,0:T(8,128)(2,1)} fusion(bf16[256,2048]{1,0:T(8,128)(2,1)S(1)} %copy-done, bf16[32,8,8,128]{3,2,1,0:T(8,128)(2,1)S(1)} %bitcast.77), kind=kOutput, calls=%fused_computation.7 | convolution fusion | flops 1075838976 | bytes 5767168 | tf_op jit(solution)/shard_map/dot_general | solution.py:113
  150.6 38.3 %reduce-scatter.2.cloned.1.call-done = bf16[128,2048]{1,0:T(8,128)(2,1)} async-done(((bf16[1024,2048]{1,0:T(8,128)(2,1)}), bf16[128,2048]{1,0:T(8,128)(2,1)}) %reduce-scatter.2.cloned.1.call-update) | async-done | bytes 524304 | tf_op jit(solution)/shard_map/reduce_scatter | solution.py:112
  (32 shorter events, 1.4 us)
Async XLA Ops:
  6.5 140.8 %copy-start = (bf16[256,2048]{1,0:T(8,128)(2,1)S(1)}, bf16[256,2048]{1,0:T(8,128)(2,1)}, u32[]{:S(2)}) copy-start(bf16[256,2048]{1,0:T(8,128)(2,1)} %param.10) | copy-start | bytes 3145732
  8.0 20.5 %all-to-all-start = ((s32[32,8,12]{2,1,0:T(8,128)}), s32[32,8,12]{2,1,0:T(8,128)S(1)}, u32[]{:S(2)}, u32[]{:S(2)}) async-start(s32[32,8,12]{2,1,0:T(8,128)} %broadcast_in_dim.20), calls=%async_computation | async-start | bytes 262144 | tf_op jit(solution)/shard_map/all_to_all | solution.py:20
  29.4 8.3 %copy-start.4 = (bf16[2048,128]{1,0:T(8,128)(2,1)S(1)}, bf16[2048,128]{1,0:T(8,128)(2,1)}, u32[]{:S(2)}) copy-start(bf16[2048,128]{1,0:T(8,128)(2,1)} %param.8) | copy-start | bytes 1572868
  31.5 55.7 %all-to-all-start.1 = ((bf16[32,8,32,128]{3,2,1,0:T(8,128)(2,1)}), bf16[32,8,32,128]{3,2,1,0:T(8,128)(2,1)}, u32[]{:S(2)}, u32[]{:S(2)}) async-start(bf16[32,8,32,128]{3,2,1,0:T(8,128)(2,1)} %bitcast.3), calls=%async_computation.1 | async-start | bytes 4194304 | tf_op jit(solution)/shard_map/all_to_all | solution.py:54
  41.1 52.0 %copy-start.3 = (s32[8,12]{1,0:T(8,128)S(1)}, s32[8,12]{1,0:T(8,128)}, u32[]{:S(2)}) copy-start(s32[8,12]{1,0:T(8,128)} %param.11) | copy-start | bytes 1156
  87.2 53.7 %all-to-all-start.2 = ((bf16[32,8,32,128]{3,2,1,0:T(8,128)(2,1)}), bf16[32,8,32,128]{3,2,1,0:T(8,128)(2,1)}, u32[]{:S(2)}, u32[]{:S(2)}) async-start(bf16[32,8,32,128]{3,2,1,0:T(8,128)(2,1)} %bitcast.76), calls=%async_computation.2 | async-start | bytes 4194304 | tf_op jit(solution)/shard_map/all_to_all | solution.py:53
  92.8 96.1 %reduce-scatter.2.cloned.1.call-start = ((), (), s32[]{:S(2)}) async-start(), calls=%async_computation.4 | async-start | bytes 4718592 | tf_op jit(solution)/shard_map/reduce_scatter | solution.py:112
  144.5 1.1 copy-start.1
  144.5 1.2 copy-start.2
Sparse Core Ops, SparseCore 0:
  150.8 38.1 reduce-scatter.1
where the time goes:
time: 196 us
  waiting for transfers between devices  125 us (64%)
  starting transfers between devices  23.5 us (12%)
  matrix products  16.1 us (8%)
  local copies, waits for them, and re-layouts  14.8 us (8%)
  between operations  13.6 us (7%)
  other arithmetic  3.09 us (2%)
    all_to_all x1, waiting for transfers between devices, shards(): lax.all_to_all(value_rows[wanted], 'kv', split_axis=0, concat_axis=0, til...  43.9 us
    reduce_scatter x1, waiting for transfers between devices, shards(): lax.psum_scatter(jnp.dot(mixed, out_weight, preferred_element_type=jnp.fl...  38.3 us
    all_to_all x1, waiting for transfers between devices, shards(): lax.all_to_all(key_rows[wanted], 'kv', split_axis=0, concat_axis=0, tiled...  37.1 us
    all_to_all x1, starting transfers between devices, from_everyone(): lax.all_to_all(jnp.broadcast_to(x[None], (size, *x.shape)), axis, 0, 0, t...  11.6 us
    all_to_all x1, starting transfers between devices, shards(): lax.all_to_all(value_rows[wanted], 'kv', split_axis=0, concat_axis=0, til...  6.12 us
    all_to_all x1, starting transfers between devices, shards(): lax.all_to_all(key_rows[wanted], 'kv', split_axis=0, concat_axis=0, tiled...  5.61 us
    all_to_all x1, waiting for transfers between devices, from_everyone(): lax.all_to_all(jnp.broadcast_to(x[None], (size, *x.shape)), axis, 0, 0, t...  5.36 us
  transfers between devices with their start and end apart: 4, of which 4 were waited for; matrix products, arithmetic and copies ran while one was open for 10% of the time, Pallas kernels for 0%

commit v1 on v0

v1 whole, which is shorter than its diff:
```python
import functools

import jax
import jax.numpy as jnp
from jax import lax
from jax.experimental import pallas as pl
from jax.experimental.pallas import tpu as pltpu
from jax.sharding import PartitionSpec as P

MESH = pl.DeviceIdType.MESH
NZ, NX, NY, NC = 8, 4, 4, 2
TP = NY * NC
HALF = NZ // 2
HEAD = 128
SPAN = 128
KSPAN = 32
NFAR = 12
TOK = 1024
NBLK = TOK // KSPAN
NQB = TOK // SPAN
WIDTH = 2048
QW = 256
GROUPS = NZ * NX
LISTED = SPAN + NFAR * KSPAN
CHUNK = 256
NCHUNK = TOK // CHUNK
SCALE = HEAD ** (-0.5)
K, V = 0, 1
UP = [(K, j) for j in range(1, HALF + 1)] + [(V, j) for j in range(1, HALF)]
DOWN = [(K, j) for j in range(1, HALF)] + [(V, j) for j in range(1, HALF + 1)]


def kernel(
    tok_h, wq_h, wk_h, wv_h, wo_h, chosen_v, chosen_s,
    out_ref,
    x_v, w_v, wfull, q_v, own_k, own_v, up_bufs, dn_bufs, uni_k, uni_v, stage,
    tab_v, tab_s, kb, vb, att, att_all, acc,
    tok_sem, w_sem, wo_sem, tab_send, tab_recv, tab_loc,
    up_send, up_recv, dn_send, dn_recv, x_send, x_recv,
    wy_send, wy_recv, wd_send, wd_recv, att_send, att_recv,
):
    kv = lax.axis_index("kv")
    tp = lax.axis_index("tp")
    z, x = kv // NX, kv % NX
    y, c = tp // NC, tp % NC

    def at_z(step):
        return {"kv": ((z + step + NZ) % NZ) * NX + x, "tp": tp}

    def at_x(step):
        return {"kv": z * NX + (x + step + NX) % NX, "tp": tp}

    def at_tp(index):
        return {"kv": kv, "tp": index}

    def tp_of(dy, dc):
        return ((y + dy + NY) % NY) * NC + (c + dc) % NC

    bar = pltpu.get_barrier_semaphore()
    for dev in [at_z(1), at_z(-1)] + [at_x(d) for d in range(1, NX)]:
        pl.semaphore_signal(bar, inc=1, device_id=dev, device_id_type=MESH)
    for d in range(1, TP):
        pl.semaphore_signal(bar, inc=1, device_id=at_tp((tp + d) % TP), device_id_type=MESH)

    def rows(i):
        return pl.ds(pl.multiple_of(i * CHUNK, CHUNK), CHUNK)

    def tok_copy(i):
        return pltpu.make_async_copy(tok_h.at[rows(i)], x_v.at[rows(i)], tok_sem.at[i])

    w_copies = [
        pltpu.make_async_copy(wk_h, w_v.at[:, 0:128], w_sem.at[0]),
        pltpu.make_async_copy(wv_h, w_v.at[:, 128:256], w_sem.at[1]),
        pltpu.make_async_copy(wq_h, w_v.at[:, 256:512], w_sem.at[2]),
    ]
    w_copies[0].start()
    w_copies[1].start()
    for i in range(NCHUNK):
        tok_copy(i).start()
    wo_copy = pltpu.make_async_copy(wo_h, wfull.at[tp], wo_sem.at[0])
    wo_copy.start()
    w_copies[2].start()

    lane = lax.broadcasted_iota(jnp.int32, (NQB, 128), 1)
    table = jnp.zeros((NQB, 128), jnp.int32)
    listed = chosen_v[...]
    for j in range(NFAR):
        col = jnp.broadcast_to(listed[:, j : j + 1], (NQB, 128))
        table = table + jnp.where((col >= 0) & ((col >> 5) == lane), col & (NBLK - 1), 0)
    tab_v[0] = table

    pl.semaphore_wait(bar, 2 + NX - 1 + TP - 1)

    def tab_copy(d):
        return pltpu.make_async_remote_copy(
            src_ref=tab_v.at[0], dst_ref=tab_v.at[d], send_sem=tab_send.at[d], recv_sem=tab_recv.at[d],
            device_id=at_x(d), device_id_type=MESH,
        )

    def tab_to_smem(d):
        return pltpu.make_async_copy(tab_v.at[d], tab_s.at[d], tab_loc.at[d])

    for d in range(1, NX):
        tab_copy(d).start()
    tab_to_smem(0).start()

    def wy(slot, sem, dy, lo, hi):
        ref = wfull.at[slot, lo:hi]
        return pltpu.make_async_remote_copy(
            src_ref=ref, dst_ref=ref, send_sem=wy_send.at[sem], recv_sem=wy_recv.at[sem],
            device_id=at_tp(tp_of(dy, 0)), device_id_type=MESH,
        )

    def wd(slot, sem, lo, hi):
        ref = wfull.at[slot, lo:hi]
        return pltpu.make_async_remote_copy(
            src_ref=ref, dst_ref=ref, send_sem=wd_send.at[sem], recv_sem=wd_recv.at[sem],
            device_id=at_tp(tp_of(0, 1)), device_id_type=MESH,
        )

    y_sends = [(tp, 0, 1, 0, QW), (tp, 1, -1, 0, QW), (tp_of(-1, 0), 2, 1, 0, QW // 2), (tp_of(1, 0), 3, -1, QW // 2, QW)]
    y_recvs = [
        (tp_of(-1, 0), 0, 1, 0, QW), (tp_of(1, 0), 1, -1, 0, QW),
        (tp_of(2, 0), 2, 1, 0, QW // 2), (tp_of(2, 0), 3, -1, QW // 2, QW),
    ]
    d_rows = [(0, QW), (0, QW), (0, QW), (0, QW // 2), (QW // 2, QW)]
    d_sends = [(s, i) + d_rows[i] for i, s in enumerate([tp, tp_of(-1, 0), tp_of(1, 0), tp_of(2, 0), tp_of(2, 0)])]
    d_recvs = [(s, i) + d_rows[i] for i, s in enumerate([tp_of(0, 1), tp_of(-1, 1), tp_of(1, 1), tp_of(2, 1), tp_of(2, 1)])]
    wo_copy.wait()
    wy(*y_sends[0]).start()
    wy(*y_sends[1]).start()
    wd(*d_sends[0]).start()

    w_copies[0].wait()
    w_copies[1].wait()

    def project_kv(i, carry):
        tok_copy(i).wait()
        pair = jnp.dot(x_v[rows(i)], w_v[:, 0:256], preferred_element_type=jnp.float32).astype(jnp.bfloat16)
        blocks = pl.ds(i * (CHUNK // KSPAN), CHUNK // KSPAN)
        own_k[blocks] = pair[:, :HEAD].reshape(CHUNK // KSPAN, KSPAN, HEAD)
        own_v[blocks] = pair[:, HEAD:].reshape(CHUNK // KSPAN, KSPAN, HEAD)
        return carry

    lax.fori_loop(0, NCHUNK, project_kv, 0)
    own = {K: own_k, V: own_v}
    up_ref = {(p, j): up_bufs[i] for i, (p, j) in enumerate(UP)}
    dn_ref = {(p, j): dn_bufs[i] for i, (p, j) in enumerate(DOWN)}
    uni = {K: uni_k, V: uni_v}

    def up_copy(p, j):
        src = own[p] if j == 1 else up_ref[p, j - 1]
        return pltpu.make_async_remote_copy(
            src_ref=src, dst_ref=up_ref[p, j], send_sem=up_send.at[p, j], recv_sem=up_recv.at[p, j],
            device_id=at_z(1), device_id_type=MESH,
        )

    def dn_copy(p, j):
        src = own[p] if j == 1 else dn_ref[p, j - 1]
        return pltpu.make_async_remote_copy(
            src_ref=src, dst_ref=dn_ref[p, j], send_sem=dn_send.at[p, j], recv_sem=dn_recv.at[p, j],
            device_id=at_z(-1), device_id_type=MESH,
        )

    def up_arrives(p, j, here):
        return (here - j >= 0) & (here <= NZ - 1)

    def dn_arrives(p, j, here):
        first = (here + j) % NZ
        return first <= (HALF - 2 if p == K else HALF - 1)

    def send_up(p, j):
        if (p, j) in up_ref:
            @pl.when(up_arrives(p, j, z + 1))
            def _():
                up_copy(p, j).start()

    def send_down(p, j):
        if (p, j) in dn_ref:
            @pl.when(dn_arrives(p, j, (z + NZ - 1) % NZ))
            def _():
                dn_copy(p, j).start()

    def stage_rows(a, p, d):
        return ((a * 2 + p) * (NX - 1) + d - 1) * NQB

    def x_copy(a, p, d, source, sender_x):
        group_rows = pl.ds((source * NX + sender_x) * NQB, NQB)
        return pltpu.make_async_remote_copy(
            src_ref=stage.at[pl.ds(stage_rows(a, p, d), NQB)],
            dst_ref=uni[p].at[group_rows],
            send_sem=x_send.at[a, p, d - 1], recv_sem=x_recv.at[a, p, d - 1],
            device_id=at_x(d), device_id_type=MESH,
        )

    def spread(a, p, buf, source, mine):
        group = source * NX + x

        def pick(b, carry):
            for d in range(1, NX):
                stage[stage_rows(a, p, d) + b] = buf[tab_s[NX - d, b, group]]
            if mine:
                uni[p][group * NQB + b] = buf[tab_s[0, b, group]]
            return carry

        lax.fori_loop(0, NQB, pick, 0)
        for d in range(1, NX):
            if mine:
                x_copy(a, p, d, source, x).start()
            else:
                @pl.when(x + d < NX)
                def _():
                    x_copy(a, p, d, source, x).start()

    for p in (K, V):
        send_up(p, 1)
        send_down(p, 1)

    for d in range(1, NX):
        tab_copy(d).wait_recv()
        tab_to_smem(d).start()
    for d in range(NX):
        tab_to_smem(d).wait()

    spread(0, K, own_k, z, False)
    spread(0, V, own_v, z, False)

    w_copies[2].wait()

    def project_q(i, carry):
        q_v[rows(i)] = jnp.dot(x_v[rows(i)], w_v[:, 256:512], preferred_element_type=jnp.float32).astype(jnp.bfloat16)
        return carry

    lax.fori_loop(0, NCHUNK, project_q, 0)

    for j in range(1, HALF + 1):
        for p in (K, V):
            if (p, j) in up_ref:
                @pl.when(up_arrives(p, j, z))
                def _():
                    up_copy(p, j).wait_recv()
                    send_up(p, j + 1)
                    spread(j, p, up_ref[p, j], z - j, True)
            if (p, j) in dn_ref:
                @pl.when(dn_arrives(p, j, z))
                def _():
                    dn_copy(p, j).wait_recv()
                    send_down(p, j + 1)

                    @pl.when(z + j >= NZ)
                    def _():
                        spread(HALF + j, p, dn_ref[p, j], z + j - NZ, True)
        if j == 2:
            for i in (0, 1):
                wy(*y_recvs[i]).wait_recv()
                wy(*y_sends[2 + i]).start()
                wd(*d_sends[1 + i]).start()
        if j == HALF:
            for i in (2, 3):
                wy(*y_recvs[i]).wait_recv()
                wd(*d_sends[1 + i]).start()

    def each_x(act):
        for p in (K, V):
            for d in range(1, NX):
                act(0, p, d, z, None)
                for j in range(1, HALF + 1):
                    if (p, j) in up_ref:
                        act(j, p, d, z - j, z - j >= 0)
                    if (p, j) in dn_ref:
                        act(HALF + j, p, d, z + j - NZ, z + j >= NZ)

    def wait_x(a, p, d, source, when):
        sender = (x + NX - d) % NX

        @pl.when(sender < x if when is None else when)
        def _():
            x_copy(a, p, d, source, sender).wait_recv()

    each_x(wait_x)

    far_count = jnp.minimum(kv, NFAR)
    row_at = lax.broadcasted_iota(jnp.int32, (2 * SPAN, LISTED), 0) & (SPAN - 1)
    col_at = lax.broadcasted_iota(jnp.int32, (2 * SPAN, LISTED), 1)
    last_at = jnp.where(col_at < SPAN, row_at, SPAN - 1 + far_count * KSPAN)

    def att_copy(b, sender):
        return pltpu.make_async_remote_copy(
            src_ref=att.at[b], dst_ref=att_all.at[sender], send_sem=att_send.at[b], recv_sem=att_recv.at[sender],
            device_id=at_tp(b), device_id_type=MESH,
        )

    def attend(i, carry):
        b = (tp + 1 + i) % TP
        kb[0:SPAN] = own_k[pl.ds(b * (SPAN // KSPAN), SPAN // KSPAN)].reshape(SPAN, HEAD)
        vb[0:SPAN] = own_v[pl.ds(b * (SPAN // KSPAN), SPAN // KSPAN)].reshape(SPAN, HEAD)
        for j in range(NFAR):
            picked = jnp.maximum(chosen_s[b, j], 0)
            at = (picked >> 5) * NQB + b
            kb[SPAN + j * KSPAN : SPAN + (j + 1) * KSPAN] = uni_k[at]
            block = uni_v[at]
            vb[SPAN + j * KSPAN : SPAN + (j + 1) * KSPAN] = jnp.where(j < far_count, block, jnp.zeros_like(block))
        q_rows = pl.ds(pl.multiple_of(b * SPAN, SPAN), SPAN)
        qs = jnp.concatenate([q_v[q_rows, 0:HEAD], q_v[q_rows, HEAD:QW]], axis=0)
        scores = lax.dot_general(qs, kb[...], (((1,), (1,)), ((), ())), preferred_element_type=jnp.float32) * SCALE
        scores = jnp.where(col_at <= last_at, scores, -jnp.inf)
        top = jnp.max(scores, axis=1, keepdims=True)
        grown = jnp.exp(scores - top)
        total = jnp.sum(grown, axis=1, keepdims=True)
        weights = (grown * (1.0 / total)).astype(jnp.bfloat16)
        mixed = jnp.dot(weights, vb[...], preferred_element_type=jnp.float32).astype(jnp.bfloat16)
        joined = jnp.concatenate([mixed[:SPAN], mixed[SPAN:]], axis=1)

        @pl.when(i < TP - 1)
        def _():
            att[b] = joined
            att_copy(b, tp).start()

        @pl.when(i == TP - 1)
        def _():
            att_all[tp] = joined

        return carry

    lax.fori_loop(0, TP, attend, 0)

    for args in d_recvs:
        wd(*args).wait_recv()

    def gather(i, carry):
        g = (tp + TP - 1 - i) % TP

        @pl.when(i < TP - 1)
        def _():
            att_copy(tp, g).wait_recv()

        part = jnp.dot(att_all[g], wfull[g], preferred_element_type=jnp.float32).astype(jnp.bfloat16).astype(jnp.float32)

        @pl.when(i == 0)
        def _():
            acc[...] = part

        @pl.when(i > 0)
        def _():
            acc[...] += part

        return carry

    lax.fori_loop(0, TP, gather, 0)
    out_ref[...] = acc[...].astype(jnp.bfloat16)

    for d in range(1, NX):
        tab_copy(d).wait_send()
    for args in y_sends:
        wy(*args).wait_send()
    for args in d_sends:
        wd(*args).wait_send()
    for (p, j) in up_ref:
        @pl.when(up_arrives(p, j, z + 1))
        def _():
            up_copy(p, j).wait_send()
    for (p, j) in dn_ref:
        @pl.when(dn_arrives(p, j, (z + NZ - 1) % NZ))
        def _():
            dn_copy(p, j).wait_send()

    def wait_sent(a, p, d, source, when):
        @pl.when(x + d < NX if when is None else when)
        def _():
            x_copy(a, p, d, source, x).wait_send()

    each_x(wait_sent)

    def att_sent(i, carry):
        b = (tp + 1 + i) % TP
        att_copy(b, tp).wait_send()
        return carry

    lax.fori_loop(0, TP - 1, att_sent, 0)


def shards(tokens, query_weight, key_projection_matrix, value_projection_matrix, out_weight, chosen):
    bf16 = jnp.bfloat16
    piece = pltpu.VMEM((NBLK, KSPAN, HEAD), bf16)
    dma = pltpu.SemaphoreType.DMA
    any_space = pl.BlockSpec(memory_space=pl.ANY)
    arrivals = 2 * HALF + 1
    return pl.pallas_call(
        kernel,
        out_shape=jax.ShapeDtypeStruct((SPAN, WIDTH), bf16),
        in_specs=[any_space] * 5 + [pl.BlockSpec(memory_space=pltpu.VMEM), pl.BlockSpec(memory_space=pltpu.SMEM)],
        out_specs=pl.BlockSpec(memory_space=pltpu.VMEM),
        scratch_shapes=[
            pltpu.VMEM((TOK, WIDTH), bf16),
            pltpu.VMEM((WIDTH, 2 * HEAD + QW), bf16),
            pltpu.VMEM((TP, QW, WIDTH), bf16),
            pltpu.VMEM((TOK, QW), bf16),
            piece,
            piece,
            [piece for _ in UP],
            [piece for _ in DOWN],
            pltpu.VMEM((GROUPS * NQB, KSPAN, HEAD), bf16),
            pltpu.VMEM((GROUPS * NQB, KSPAN, HEAD), bf16),
            pltpu.VMEM((arrivals * 2 * (NX - 1) * NQB, KSPAN, HEAD), bf16),
            pltpu.VMEM((NX, NQB, 128), jnp.int32),
            pltpu.SMEM((NX, NQB, 128), jnp.int32),
            pltpu.VMEM((LISTED, HEAD), bf16),
            pltpu.VMEM((LISTED, HEAD), bf16),
            pltpu.VMEM((TP, SPAN, QW), bf16),
            pltpu.VMEM((TP, SPAN, QW), bf16),
            pltpu.VMEM((SPAN, WIDTH), jnp.float32),
            dma((NCHUNK,)), dma((3,)), dma((1,)), dma((NX,)), dma((NX,)), dma((NX,)),
            dma((2, HALF + 1)), dma((2, HALF + 1)), dma((2, HALF + 1)), dma((2, HALF + 1)),
            dma((arrivals, 2, NX - 1)), dma((arrivals, 2, NX - 1)),
            dma((4,)), dma((4,)), dma((5,)), dma((5,)), dma((TP,)), dma((TP,)),
        ],
        compiler_params=pltpu.CompilerParams(
            collective_id=0, has_side_effects=True, vmem_limit_bytes=56 * 2**20
        ),
        name="sparse_attention_layer",
    )(tokens, query_weight, key_projection_matrix, value_projection_matrix, out_weight, chosen, chosen)


def solution(mesh):
    return jax.shard_map(
        shards,
        mesh=mesh,
        in_specs=(
            P("kv", None),
            P(None, "tp"),
            P(None, "tp"),
            P(None, "tp"),
            P("tp", None),
            P("kv", None),
        ),
        out_specs=P(("kv", "tp"), None),
        check_vma=False,
    )
```

time: 196 us -> 71 us (0.36)
  the two profiles are of different devices: /device:TPU:6 before, /device:TPU:193 now
where the time goes in v1:
time: 71 us; the launch traced here: 70.8 us
  Pallas kernels  68.9 us (97%)
  local copies, waits for them, and re-layouts  1.88 us (3%)
    pallas_call x1, Pallas kernels, shards(): pl.pallas_call(kernel, out_shape=jax.ShapeDtypeStruct((SPAN, WIDTH), bf16...  68.9 us
    unnamed x1, local copies, waits for them, and re-layouts  1.88 us

profile of v1, /device:TPU:193, one launch (start us, length us, event | category | flops | bytes accessed | tf_op | source)
XLA Modules:
  0.0 70.8 jit_solution(11811403355372393344)
XLA Ops:
  0.0 68.9 %sparse_attention_layer.1 = bf16[128,2048]{1,0:T(8,128)(2,1)} custom-call(bf16[1024,2048]{1,0:T(8,128)(2,1)} %tok_h.1, bf16[2048,256]{1,0:T(8,128)(2,1)} %wq_h.1, bf16[2048,128]{1,0:T(8,128)(2,1)} %wk_h.1, bf16[2048,128]{1,0:T(8,128)(2,1)} %wv_h.1, bf16[256,2048]{1,0:T(8,128)(2,1)} %wo_h.1, s32[8,12]{1,0:T(8,128)} %chosen_s.1, s32[8,12]{1,0:T(8,128)} %chosen_s.1), custom_call_target="tpu_custom_call" | custom-call | tf_op jit(solution)/shard_map/sparse_attention_layer/pallas_call | solution.py:388
  68.9 1.9 %copy.8 = bf16[128,2048]{1,0:T(8,128)(2,1)} copy(bf16[128,2048]{1,0:T(8,128)(2,1)} %sparse_attention_layer.1) | data formatting | bytes 1048576

commit v2 on v1

--- a/solution.py
+++ b/solution.py
@@ -24,19 +24,21 @@
 LISTED = SPAN + NFAR * KSPAN
 CHUNK = 256
 NCHUNK = TOK // CHUNK
-SCALE = HEAD ** (-0.5)
+LOG_SCALE = HEAD ** (-0.5) * 1.4426950408889634
 K, V = 0, 1
-UP = [(K, j) for j in range(1, HALF + 1)] + [(V, j) for j in range(1, HALF)]
+UP = [(p, j) for j in range(1, HALF) for p in (K, V)]
 DOWN = [(K, j) for j in range(1, HALF)] + [(V, j) for j in range(1, HALF + 1)]
+LAST = NZ - 1
 
 
 def kernel(
-    tok_h, wq_h, wk_h, wv_h, wo_h, chosen_v, chosen_s,
+    tok_h, wq_h, wk_h, wv_h, wo_h, chosen_h,
     out_ref,
-    x_v, w_v, wfull, q_v, own_k, own_v, up_bufs, dn_bufs, uni_k, uni_v, stage,
+    chosen_v, chosen_s, chosen_sem,
+    x_v, w_v, wfull, q_v, own_k, own_v, up_bufs, dn_bufs, uni_k, uni_v, stage, relay_bufs, relay_stage,
     tab_v, tab_s, kb, vb, att, att_all, acc,
     tok_sem, w_sem, wo_sem, tab_send, tab_recv, tab_loc,
-    up_send, up_recv, dn_send, dn_recv, x_send, x_recv,
+    up_send, up_recv, dn_send, dn_recv, x_send, x_recv, r_send, r_recv,
     wy_send, wy_recv, wd_send, wd_recv, att_send, att_recv,
 ):
     kv = lax.axis_index("kv")
@@ -50,6 +52,9 @@
     def at_x(step):
         return {"kv": z * NX + (x + step + NX) % NX, "tp": tp}
 
+    def at_zx(dz, dx):
+        return {"kv": ((z + dz + NZ) % NZ) * NX + (x + dx) % NX, "tp": tp}
+
     def at_tp(index):
         return {"kv": kv, "tp": index}
 
@@ -57,10 +62,17 @@
         return ((y + dy + NY) % NY) * NC + (c + dc) % NC
 
     bar = pltpu.get_barrier_semaphore()
-    for dev in [at_z(1), at_z(-1)] + [at_x(d) for d in range(1, NX)]:
+    for dev in [at_zx(dz, d) for dz in (1, -1) for d in range(NX)] + [at_x(d) for d in range(1, NX)]:
         pl.semaphore_signal(bar, inc=1, device_id=dev, device_id_type=MESH)
     for d in range(1, TP):
         pl.semaphore_signal(bar, inc=1, device_id=at_tp((tp + d) % TP), device_id_type=MESH)
+
+    listed_copies = [
+        pltpu.make_async_copy(chosen_h, chosen_v, chosen_sem.at[0]),
+        pltpu.make_async_copy(chosen_h, chosen_s, chosen_sem.at[1]),
+    ]
+    for copy in listed_copies:
+        copy.start()
 
     def rows(i):
         return pl.ds(pl.multiple_of(i * CHUNK, CHUNK), CHUNK)
@@ -83,13 +95,28 @@
 
     lane = lax.broadcasted_iota(jnp.int32, (NQB, 128), 1)
     table = jnp.zeros((NQB, 128), jnp.int32)
+    for copy in listed_copies:
+        copy.wait()
     listed = chosen_v[...]
     for j in range(NFAR):
         col = jnp.broadcast_to(listed[:, j : j + 1], (NQB, 128))
         table = table + jnp.where((col >= 0) & ((col >> 5) == lane), col & (NBLK - 1), 0)
     tab_v[0] = table
 
-    pl.semaphore_wait(bar, 2 + NX - 1 + TP - 1)
+    w_copies[0].wait()
+    w_copies[1].wait()
+
+    def project_kv(i, carry):
+        tok_copy(i).wait()
+        pair = jnp.dot(x_v[rows(i)], w_v[:, 0:256], preferred_element_type=jnp.float32).astype(jnp.bfloat16)
+        blocks = pl.ds(i * (CHUNK // KSPAN), CHUNK // KSPAN)
+        own_k[blocks] = pair[:, :HEAD].reshape(CHUNK // KSPAN, KSPAN, HEAD)
+        own_v[blocks] = pair[:, HEAD:].reshape(CHUNK // KSPAN, KSPAN, HEAD)
+        return carry
+
+    lax.fori_loop(0, NCHUNK, project_kv, 0)
+
+    pl.semaphore_wait(bar, 2 * NX + NX - 1 + TP - 1)
 
     def tab_copy(d):
         return pltpu.make_async_remote_copy(
@@ -100,8 +127,26 @@
     def tab_to_smem(d):
         return pltpu.make_async_copy(tab_v.at[d], tab_s.at[d], tab_loc.at[d])
 
+    def tab_relay_copy(d, dz):
+        return pltpu.make_async_remote_copy(
+            src_ref=tab_v.at[0], dst_ref=tab_v.at[NX + d], send_sem=tab_send.at[NX * (1 if dz < 0 else 2) + d],
+            recv_sem=tab_recv.at[NX + d], device_id=at_zx(dz, d), device_id_type=MESH,
+        )
+
+    relays = (z == 0) | ((z >= HALF - 2) & (z <= LAST - 1))
     for d in range(1, NX):
         tab_copy(d).start()
+
+    @pl.when(z >= HALF - 1)
+    def _():
+        for d in range(NX):
+            tab_relay_copy(d, -1).start()
+
+    @pl.when(z == LAST)
+    def _():
+        for d in range(NX):
+            tab_relay_copy(d, 1).start()
+
     tab_to_smem(0).start()
 
     def wy(slot, sem, dy, lo, hi):
@@ -131,18 +176,6 @@
     wy(*y_sends[1]).start()
     wd(*d_sends[0]).start()
 
-    w_copies[0].wait()
-    w_copies[1].wait()
-
-    def project_kv(i, carry):
-        tok_copy(i).wait()
-        pair = jnp.dot(x_v[rows(i)], w_v[:, 0:256], preferred_element_type=jnp.float32).astype(jnp.bfloat16)
-        blocks = pl.ds(i * (CHUNK // KSPAN), CHUNK // KSPAN)
-        own_k[blocks] = pair[:, :HEAD].reshape(CHUNK // KSPAN, KSPAN, HEAD)
-        own_v[blocks] = pair[:, HEAD:].reshape(CHUNK // KSPAN, KSPAN, HEAD)
-        return carry
-
-    lax.fori_loop(0, NCHUNK, project_kv, 0)
     own = {K: own_k, V: own_v}
     up_ref = {(p, j): up_bufs[i] for i, (p, j) in enumerate(UP)}
     dn_ref = {(p, j): dn_bufs[i] for i, (p, j) in enumerate(DOWN)}
@@ -163,11 +196,15 @@
         )
 
     def up_arrives(p, j, here):
-        return (here - j >= 0) & (here <= NZ - 1)
+        first = LAST if (p, j) == (V, HALF - 1) else j
+        return (here >= first) & (here <= LAST)
 
     def dn_arrives(p, j, here):
-        first = (here + j) % NZ
-        return first <= (HALF - 2 if p == K else HALF - 1)
+        source = (here + j) % NZ
+        lands = source <= (HALF - 2 if p == K else HALF - 1)
+        if (p, j) in ((K, HALF - 1), (V, HALF)):
+            lands = lands & (here != LAST)
+        return lands
 
     def send_up(p, j):
         if (p, j) in up_ref:
@@ -181,14 +218,63 @@
             def _():
                 dn_copy(p, j).start()
 
-    def stage_rows(a, p, d):
-        return ((a * 2 + p) * (NX - 1) + d - 1) * NQB
+    RELAYS = [
+        (0, V, HALF - 2, 1, HALF - 2, LAST - 2),
+        (1, K, HALF - 1, 1, HALF - 1, LAST - 1),
+        (0, K, HALF - 2, -1, 0, 0),
+        (1, V, HALF - 1, -1, 0, 0),
+    ]
+
+    def relay_x_copy(slot, d, sender_x):
+        return pltpu.make_async_remote_copy(
+            src_ref=relay_stage.at[slot * (NX - 1) + d - 1], dst_ref=relay_bufs[slot].at[sender_x],
+            send_sem=r_send.at[slot, d], recv_sem=r_recv.at[slot, d],
+            device_id=at_x(d), device_id_type=MESH,
+        )
+
+    def relay_z_copy(slot, p, j, dz, source):
+        sems = (up_send, up_recv) if dz == 1 else (dn_send, dn_recv)
+        return pltpu.make_async_remote_copy(
+            src_ref=relay_bufs[slot], dst_ref=uni[p].at[pl.ds(source * NX, NX)],
+            send_sem=sems[0].at[p, j], recv_sem=sems[1].at[p, j],
+            device_id=at_z(dz), device_id_type=MESH,
+        )
+
+    def relay_begin(slot, p, buf, source):
+        group = source * NX + x
+
+        def pick(i, carry):
+            b = (tp + 1 + i) % TP
+            for d in range(NX):
+                block = buf[tab_s[NX + (NX - d) % NX, b, group]]
+                if d == 0:
+                    relay_bufs[slot][x, i] = block
+                else:
+                    relay_stage[slot * (NX - 1) + d - 1, i] = block
+            return carry
+
+        lax.fori_loop(0, NQB, pick, 0)
+        for d in range(1, NX):
+            relay_x_copy(slot, d, x).start()
+
+    def relay_end(slot, p, j, dz, source):
+        for d in range(1, NX):
+            relay_x_copy(slot, d, (x + NX - d) % NX).wait_recv()
+        relay_z_copy(slot, p, j + 1, dz, source).start()
+
+    def relay_for(p, j, dz):
+        for slot, rp, rj, rdz, low, high in RELAYS:
+            if (rp, rj, rdz) == (p, j, dz):
+                return slot, (z >= low) & (z <= high)
+        return None
+
+    def stage_at(a, p, d):
+        return (a * 2 + p) * (NX - 1) + d - 1
 
     def x_copy(a, p, d, source, sender_x):
-        group_rows = pl.ds((source * NX + sender_x) * NQB, NQB)
-        return pltpu.make_async_remote_copy(
-            src_ref=stage.at[pl.ds(stage_rows(a, p, d), NQB)],
-            dst_ref=uni[p].at[group_rows],
+        return pltpu.make_async_remote_copy(
+            src_ref=stage.at[stage_at(a, p, d)],
+            dst_ref=uni[p].at[source * NX + sender_x],
             send_sem=x_send.at[a, p, d - 1], recv_sem=x_recv.at[a, p, d - 1],
             device_id=at_x(d), device_id_type=MESH,
         )
@@ -196,11 +282,12 @@
     def spread(a, p, buf, source, mine):
         group = source * NX + x
 
-        def pick(b, carry):
+        def pick(i, carry):
+            b = (tp + 1 + i) % TP
             for d in range(1, NX):
-                stage[stage_rows(a, p, d) + b] = buf[tab_s[NX - d, b, group]]
+                stage[stage_at(a, p, d), i] = buf[tab_s[NX - d, b, group]]
             if mine:
-                uni[p][group * NQB + b] = buf[tab_s[0, b, group]]
+                uni[p][group, i] = buf[tab_s[0, b, group]]
             return carry
 
         lax.fori_loop(0, NQB, pick, 0)
@@ -222,6 +309,14 @@
     for d in range(NX):
         tab_to_smem(d).wait()
 
+    @pl.when(relays)
+    def _():
+        for d in range(NX):
+            tab_relay_copy(d, -1).wait_recv()
+            tab_to_smem(NX + d).start()
+        for d in range(NX):
+            tab_to_smem(NX + d).wait()
+
     spread(0, K, own_k, z, False)
     spread(0, V, own_v, z, False)
 
@@ -240,16 +335,31 @@
                 def _():
                     up_copy(p, j).wait_recv()
                     send_up(p, j + 1)
+                    found = relay_for(p, j, 1)
+                    if found:
+                        @pl.when(found[1])
+                        def _():
+                            relay_begin(found[0], p, up_ref[p, j], z - j)
                     spread(j, p, up_ref[p, j], z - j, True)
             if (p, j) in dn_ref:
                 @pl.when(dn_arrives(p, j, z))
                 def _():
                     dn_copy(p, j).wait_recv()
                     send_down(p, j + 1)
+                    found = relay_for(p, j, -1)
+                    if found:
+                        @pl.when(found[1])
+                        def _():
+                            relay_begin(found[0], p, dn_ref[p, j], z + j)
 
                     @pl.when(z + j >= NZ)
                     def _():
                         spread(HALF + j, p, dn_ref[p, j], z + j - NZ, True)
+        for slot, p, rj, dz, low, high in RELAYS:
+            if rj == j:
+                @pl.when((z >= low) & (z <= high))
+                def _():
+                    relay_end(slot, p, rj, dz, z - rj if dz == 1 else z + rj)
         if j == 2:
             for i in (0, 1):
                 wy(*y_recvs[i]).wait_recv()
@@ -260,15 +370,26 @@
                 wy(*y_recvs[i]).wait_recv()
                 wd(*d_sends[1 + i]).start()
 
+    divided = [
+        (0, V, HALF - 1, 1, (z >= HALF - 1) & (z <= LAST - 1)),
+        (1, K, HALF, 1, z >= HALF),
+        (0, K, HALF - 1, -1, z == LAST),
+        (1, V, HALF, -1, z == LAST),
+    ]
+    for slot, p, j, dz, when in divided:
+        @pl.when(when)
+        def _():
+            relay_z_copy(slot, p, j, dz, z - j if dz == 1 else z + j - NZ).wait_recv()
+
     def each_x(act):
         for p in (K, V):
             for d in range(1, NX):
                 act(0, p, d, z, None)
                 for j in range(1, HALF + 1):
                     if (p, j) in up_ref:
-                        act(j, p, d, z - j, z - j >= 0)
+                        act(j, p, d, z - j, up_arrives(p, j, z))
                     if (p, j) in dn_ref:
-                        act(HALF + j, p, d, z + j - NZ, z + j >= NZ)
+                        act(HALF + j, p, d, z + j - NZ, dn_arrives(p, j, z) & (z + j >= NZ))
 
     def wait_x(a, p, d, source, when):
         sender = (x + NX - d) % NX
@@ -280,9 +401,9 @@
     each_x(wait_x)
 
     far_count = jnp.minimum(kv, NFAR)
-    row_at = lax.broadcasted_iota(jnp.int32, (2 * SPAN, LISTED), 0) & (SPAN - 1)
-    col_at = lax.broadcasted_iota(jnp.int32, (2 * SPAN, LISTED), 1)
-    last_at = jnp.where(col_at < SPAN, row_at, SPAN - 1 + far_count * KSPAN)
+    near_row = lax.broadcasted_iota(jnp.int32, (2 * SPAN, SPAN), 0) & (SPAN - 1)
+    near_col = lax.broadcasted_iota(jnp.int32, (2 * SPAN, SPAN), 1)
+    far_col = lax.broadcasted_iota(jnp.int32, (2 * SPAN, NFAR * KSPAN), 1)
 
     def att_copy(b, sender):
         return pltpu.make_async_remote_copy(
@@ -290,67 +411,76 @@
             device_id=at_tp(b), device_id_type=MESH,
         )
 
-    def attend(i, carry):
+    def attend_block(i, kb, vb):
         b = (tp + 1 + i) % TP
         kb[0:SPAN] = own_k[pl.ds(b * (SPAN // KSPAN), SPAN // KSPAN)].reshape(SPAN, HEAD)
         vb[0:SPAN] = own_v[pl.ds(b * (SPAN // KSPAN), SPAN // KSPAN)].reshape(SPAN, HEAD)
         for j in range(NFAR):
             picked = jnp.maximum(chosen_s[b, j], 0)
-            at = (picked >> 5) * NQB + b
-            kb[SPAN + j * KSPAN : SPAN + (j + 1) * KSPAN] = uni_k[at]
-            block = uni_v[at]
+            kb[SPAN + j * KSPAN : SPAN + (j + 1) * KSPAN] = uni_k[picked >> 5, i]
+            block = uni_v[picked >> 5, i]
             vb[SPAN + j * KSPAN : SPAN + (j + 1) * KSPAN] = jnp.where(j < far_count, block, jnp.zeros_like(block))
         q_rows = pl.ds(pl.multiple_of(b * SPAN, SPAN), SPAN)
         qs = jnp.concatenate([q_v[q_rows, 0:HEAD], q_v[q_rows, HEAD:QW]], axis=0)
-        scores = lax.dot_general(qs, kb[...], (((1,), (1,)), ((), ())), preferred_element_type=jnp.float32) * SCALE
-        scores = jnp.where(col_at <= last_at, scores, -jnp.inf)
+        scores = lax.dot_general(qs, kb[...], (((1,), (1,)), ((), ())), preferred_element_type=jnp.float32)
+        near = jnp.where(near_col <= near_row, scores[:, :SPAN], -jnp.inf)
+        far = jnp.where(far_col < far_count * KSPAN, scores[:, SPAN:], -jnp.inf)
+        scores = jnp.concatenate([near, far], axis=1) * LOG_SCALE
         top = jnp.max(scores, axis=1, keepdims=True)
-        grown = jnp.exp(scores - top)
+        grown = jnp.exp2(scores - top)
         total = jnp.sum(grown, axis=1, keepdims=True)
         weights = (grown * (1.0 / total)).astype(jnp.bfloat16)
         mixed = jnp.dot(weights, vb[...], preferred_element_type=jnp.float32).astype(jnp.bfloat16)
-        joined = jnp.concatenate([mixed[:SPAN], mixed[SPAN:]], axis=1)
-
-        @pl.when(i < TP - 1)
-        def _():
-            att[b] = joined
-            att_copy(b, tp).start()
-
-        @pl.when(i == TP - 1)
-        def _():
-            att_all[tp] = joined
+        return jnp.concatenate([mixed[:SPAN], mixed[SPAN:]], axis=1)
+
+    def attend(i, carry):
+        first, second = (tp + 1 + 2 * i) % TP, (tp + 2 + 2 * i) % TP
+        one = attend_block(2 * i, kb.at[0], vb.at[0])
+        two = attend_block(2 * i + 1, kb.at[1], vb.at[1])
+        att[first] = one
+        att[second] = two
+        att_copy(first, tp).start()
+
+        @pl.when(i < TP // 2 - 1)
+        def _():
+            att_copy(second, tp).start()
 
         return carry
 
-    lax.fori_loop(0, TP, attend, 0)
+    lax.fori_loop(0, TP // 2, attend, 0)
 
     for args in d_recvs:
         wd(*args).wait_recv()
 
+    def part_of(piece, g):
+        return jnp.dot(piece, wfull[g], preferred_element_type=jnp.float32).astype(jnp.bfloat16).astype(jnp.float32)
+
     def gather(i, carry):
-        g = (tp + TP - 1 - i) % TP
-
-        @pl.when(i < TP - 1)
-        def _():
-            att_copy(tp, g).wait_recv()
-
-        part = jnp.dot(att_all[g], wfull[g], preferred_element_type=jnp.float32).astype(jnp.bfloat16).astype(jnp.float32)
-
-        @pl.when(i == 0)
-        def _():
-            acc[...] = part
-
-        @pl.when(i > 0)
-        def _():
-            acc[...] += part
-
+        g, h = (tp + TP - 1 - 2 * i) % TP, (tp + TP - 2 - 2 * i) % TP
+        att_copy(tp, g).wait_recv()
+        att_copy(tp, h).wait_recv()
+        acc[...] += part_of(att_all[g], g) + part_of(att_all[h], h)
         return carry
 
-    lax.fori_loop(0, TP, gather, 0)
-    out_ref[...] = acc[...].astype(jnp.bfloat16)
+    acc[...] = part_of(att[tp], tp)
+    lax.fori_loop(0, TP // 2 - 1, gather, 0)
+    last = (tp + 1) % TP
+    att_copy(tp, last).wait_recv()
+    out_ref[...] = (acc[...] + part_of(att_all[last], last)).astype(jnp.bfloat16)
 
     for d in range(1, NX):
         tab_copy(d).wait_send()
+
+    @pl.when(z >= HALF - 1)
+    def _():
+        for d in range(NX):
+            tab_relay_copy(d, -1).wait_send()
+
+    @pl.when(z == LAST)
+    def _():
+        for d in range(NX):
+            tab_relay_copy(d, 1).wait_send()
+
     for args in y_sends:
         wy(*args).wait_send()
     for args in d_sends:
@@ -363,6 +493,13 @@
         @pl.when(dn_arrives(p, j, (z + NZ - 1) % NZ))
         def _():
             dn_copy(p, j).wait_send()
+
+    for slot, p, rj, dz, low, high in RELAYS:
+        @pl.when((z >= low) & (z <= high))
+        def _():
+            for d in range(1, NX):
+                relay_x_copy(slot, d, x).wait_send()
+            relay_z_copy(slot, p, rj + 1, dz, z - rj if dz == 1 else z + rj).wait_send()
 
     def wait_sent(a, p, d, source, when):
         @pl.when(x + d < NX if when is None else when)
@@ -388,9 +525,12 @@
     return pl.pallas_call(
         kernel,
         out_shape=jax.ShapeDtypeStruct((SPAN, WIDTH), bf16),
-        in_specs=[any_space] * 5 + [pl.BlockSpec(memory_space=pltpu.VMEM), pl.BlockSpec(memory_space=pltpu.SMEM)],
+        in_specs=[any_space] * 6,
         out_specs=pl.BlockSpec(memory_space=pltpu.VMEM),
         scratch_shapes=[
+            pltpu.VMEM((NQB, NFAR), jnp.int32),
+            pltpu.SMEM((NQB, NFAR), jnp.int32),
+            dma((2,)),
             pltpu.VMEM((TOK, WIDTH), bf16),
             pltpu.VMEM((WIDTH, 2 * HEAD + QW), bf16),
             pltpu.VMEM((TP, QW, WIDTH), bf16),
@@ -399,26 +539,28 @@
             piece,
             [piece for _ in UP],
             [piece for _ in DOWN],
-            pltpu.VMEM((GROUPS * NQB, KSPAN, HEAD), bf16),
-            pltpu.VMEM((GROUPS * NQB, KSPAN, HEAD), bf16),
-            pltpu.VMEM((arrivals * 2 * (NX - 1) * NQB, KSPAN, HEAD), bf16),
-            pltpu.VMEM((NX, NQB, 128), jnp.int32),
-            pltpu.SMEM((NX, NQB, 128), jnp.int32),
-            pltpu.VMEM((LISTED, HEAD), bf16),
-            pltpu.VMEM((LISTED, HEAD), bf16),
+            pltpu.VMEM((GROUPS, NQB, KSPAN, HEAD), bf16),
+            pltpu.VMEM((GROUPS, NQB, KSPAN, HEAD), bf16),
+            pltpu.VMEM((arrivals * 2 * (NX - 1), NQB, KSPAN, HEAD), bf16),
+            [pltpu.VMEM((NX, NQB, KSPAN, HEAD), bf16) for _ in range(2)],
+            pltpu.VMEM((2 * (NX - 1), NQB, KSPAN, HEAD), bf16),
+            pltpu.VMEM((2 * NX, NQB, 128), jnp.int32),
+            pltpu.SMEM((2 * NX, NQB, 128), jnp.int32),
+            pltpu.VMEM((2, LISTED, HEAD), bf16),
+            pltpu.VMEM((2, LISTED, HEAD), bf16),
             pltpu.VMEM((TP, SPAN, QW), bf16),
             pltpu.VMEM((TP, SPAN, QW), bf16),
             pltpu.VMEM((SPAN, WIDTH), jnp.float32),
-            dma((NCHUNK,)), dma((3,)), dma((1,)), dma((NX,)), dma((NX,)), dma((NX,)),
+            dma((NCHUNK,)), dma((3,)), dma((1,)), dma((3 * NX,)), dma((2 * NX,)), dma((2 * NX,)),
             dma((2, HALF + 1)), dma((2, HALF + 1)), dma((2, HALF + 1)), dma((2, HALF + 1)),
-            dma((arrivals, 2, NX - 1)), dma((arrivals, 2, NX - 1)),
+            dma((arrivals, 2, NX - 1)), dma((arrivals, 2, NX - 1)), dma((2, NX)), dma((2, NX)),
             dma((4,)), dma((4,)), dma((5,)), dma((5,)), dma((TP,)), dma((TP,)),
         ],
         compiler_params=pltpu.CompilerParams(
             collective_id=0, has_side_effects=True, vmem_limit_bytes=56 * 2**20
         ),
         name="sparse_attention_layer",
-    )(tokens, query_weight, key_projection_matrix, value_projection_matrix, out_weight, chosen, chosen)
+    )(tokens, query_weight, key_projection_matrix, value_projection_matrix, out_weight, chosen)
 
 
 def solution(mesh):

time: 71 us -> 67.4 us (0.949)
  Pallas kernels: 68.9 us -> 65.4 us
    pallas_call x1, Pallas kernels: 68.9 us -> 65.4 us  [shards(): pl.pallas_call(kernel, out_shape=jax.ShapeDtypeStruct((SPAN, WIDTH), bf16...]
where the time goes in v2:
time: 67.4 us; the launch traced here: 67.3 us
  Pallas kernels  65.4 us (97%)
  local copies, waits for them, and re-layouts  1.88 us (3%)
    pallas_call x1, Pallas kernels, shards(): pl.pallas_call(kernel, out_shape=jax.ShapeDtypeStruct((SPAN, WIDTH), bf16...  65.4 us
    unnamed x1, local copies, waits for them, and re-layouts  1.88 us

profile of v2, /device:TPU:193, one launch (start us, length us, event | category | flops | bytes accessed | tf_op | source)
XLA Modules:
  0.0 67.3 jit_solution(9369083255677974031)
XLA Ops:
  0.0 65.4 %sparse_attention_layer.1 = bf16[128,2048]{1,0:T(8,128)(2,1)} custom-call(bf16[1024,2048]{1,0:T(8,128)(2,1)} %tok_h.1, bf16[2048,256]{1,0:T(8,128)(2,1)} %wq_h.1, bf16[2048,128]{1,0:T(8,128)(2,1)} %wk_h.1, bf16[2048,128]{1,0:T(8,128)(2,1)} %wv_h.1, bf16[256,2048]{1,0:T(8,128)(2,1)} %wo_h.1, s32[8,12]{1,0:T(8,128)} %chosen_h.1), custom_call_target="tpu_custom_call" | custom-call | tf_op jit(solution)/shard_map/sparse_attention_layer/pallas_call | solution.py:525
  65.4 1.9 %copy.8 = bf16[128,2048]{1,0:T(8,128)(2,1)} copy(bf16[128,2048]{1,0:T(8,128)(2,1)} %sparse_attention_layer.1) | data formatting | bytes 1048576

commit v3 on v2

--- a/solution.py
+++ b/solution.py
@@ -29,16 +29,18 @@
 UP = [(p, j) for j in range(1, HALF) for p in (K, V)]
 DOWN = [(K, j) for j in range(1, HALF)] + [(V, j) for j in range(1, HALF + 1)]
 LAST = NZ - 1
+LATE = {(HALF - 1, K): 0, (HALF - 1, V): 1, (2 * HALF - 1, K): 2, (2 * HALF, V): 3}
+FIRST = NQB // 2
 
 
 def kernel(
     tok_h, wq_h, wk_h, wv_h, wo_h, chosen_h,
     out_ref,
     chosen_v, chosen_s, chosen_sem,
-    x_v, w_v, wfull, q_v, own_k, own_v, up_bufs, dn_bufs, uni_k, uni_v, stage, relay_bufs, relay_stage,
+    x_v, w_v, wfull, q_v, own_k, own_v, up_bufs, dn_bufs, uni_k, uni_v, stage, relay_bufs, relay_stage, late_x, late_relay,
     tab_v, tab_s, kb, vb, att, att_all, acc,
     tok_sem, w_sem, wo_sem, tab_send, tab_recv, tab_loc,
-    up_send, up_recv, dn_send, dn_recv, x_send, x_recv, r_send, r_recv,
+    up_send, up_recv, dn_send, dn_recv, x_send, x_recv, xl_send, xl_recv, r_send, r_recv, rl_send, rl_recv,
     wy_send, wy_recv, wd_send, wd_recv, att_send, att_recv,
 ):
     kv = lax.axis_index("kv")
@@ -60,6 +62,13 @@
 
     def tp_of(dy, dc):
         return ((y + dy + NY) % NY) * NC + (c + dc) % NC
+
+    def block_at(i, way):
+        r, k = i // 2, i % 2
+        dy = 2 - (r + 1) // 2
+        dy = dy + k * (NY - 2 * dy)
+        dc = r // 2 + k * ((r + 1) % 2 - r // 2)
+        return ((y + way * dy + NY) % NY) * NC + (c + dc) % NC
 
     bar = pltpu.get_barrier_semaphore()
     for dev in [at_zx(dz, d) for dz in (1, -1) for d in range(NX)] + [at_x(d) for d in range(1, NX)]:
@@ -232,11 +241,14 @@
             device_id=at_x(d), device_id_type=MESH,
         )
 
-    def relay_z_copy(slot, p, j, dz, source):
-        sems = (up_send, up_recv) if dz == 1 else (dn_send, dn_recv)
-        return pltpu.make_async_remote_copy(
-            src_ref=relay_bufs[slot], dst_ref=uni[p].at[pl.ds(source * NX, NX)],
-            send_sem=sems[0].at[p, j], recv_sem=sems[1].at[p, j],
+    def relay_z_copy(slot, p, j, dz, source, second=False):
+        send, recv = (up_send, up_recv) if dz == 1 else (dn_send, dn_recv)
+        send, recv = (rl_send.at[p], rl_recv.at[p]) if second else (send.at[p, j], recv.at[p, j])
+        part = slice(0, NQB) if slot == 0 else slice(FIRST, NQB) if second else slice(0, FIRST)
+        return pltpu.make_async_remote_copy(
+            src_ref=relay_bufs[slot].at[:, part],
+            dst_ref=late_relay[p] if second else uni[p].at[pl.ds(source * NX, NX), part],
+            send_sem=send, recv_sem=recv,
             device_id=at_z(dz), device_id_type=MESH,
         )
 
@@ -244,7 +256,7 @@
         group = source * NX + x
 
         def pick(i, carry):
-            b = (tp + 1 + i) % TP
+            b = block_at(i, 1)
             for d in range(NX):
                 block = buf[tab_s[NX + (NX - d) % NX, b, group]]
                 if d == 0:
@@ -261,6 +273,8 @@
         for d in range(1, NX):
             relay_x_copy(slot, d, (x + NX - d) % NX).wait_recv()
         relay_z_copy(slot, p, j + 1, dz, source).start()
+        if slot == 1:
+            relay_z_copy(slot, p, j + 1, dz, source, True).start()
 
     def relay_for(p, j, dz):
         for slot, rp, rj, rdz, low, high in RELAYS:
@@ -271,11 +285,14 @@
     def stage_at(a, p, d):
         return (a * 2 + p) * (NX - 1) + d - 1
 
-    def x_copy(a, p, d, source, sender_x):
-        return pltpu.make_async_remote_copy(
-            src_ref=stage.at[stage_at(a, p, d)],
-            dst_ref=uni[p].at[source * NX + sender_x],
-            send_sem=x_send.at[a, p, d - 1], recv_sem=x_recv.at[a, p, d - 1],
+    def x_copy(a, p, d, source, sender_x, second=False):
+        late = LATE.get((a, p))
+        part = slice(0, NQB) if late is None else slice(FIRST, NQB) if second else slice(0, FIRST)
+        return pltpu.make_async_remote_copy(
+            src_ref=stage.at[stage_at(a, p, d), part],
+            dst_ref=late_x[late][d - 1] if second else uni[p].at[source * NX + sender_x, part],
+            send_sem=xl_send.at[late, d - 1] if second else x_send.at[a, p, d - 1],
+            recv_sem=xl_recv.at[late, d - 1] if second else x_recv.at[a, p, d - 1],
             device_id=at_x(d), device_id_type=MESH,
         )
 
@@ -283,7 +300,7 @@
         group = source * NX + x
 
         def pick(i, carry):
-            b = (tp + 1 + i) % TP
+            b = block_at(i, 1)
             for d in range(1, NX):
                 stage[stage_at(a, p, d), i] = buf[tab_s[NX - d, b, group]]
             if mine:
@@ -299,9 +316,20 @@
                 def _():
                     x_copy(a, p, d, source, x).start()
 
+    def each_x(act, second=False):
+        for p in (K, V):
+            for d in range(1, NX):
+                for a, source, when in [(0, z, None)] + [
+                    (j, z - j, up_arrives(p, j, z)) for j in range(1, HALF + 1) if (p, j) in up_ref
+                ] + [
+                    (HALF + j, z + j - NZ, dn_arrives(p, j, z) & (z + j >= NZ)) for j in range(1, HALF + 1) if (p, j) in dn_ref
+                ]:
+                    if not second or (a, p) in LATE:
+                        act(a, p, d, source, when, second)
+
     for p in (K, V):
         send_up(p, 1)
-        send_down(p, 1)
+        send_down(1 - p, 1)
 
     for d in range(1, NX):
         tab_copy(d).wait_recv()
@@ -328,38 +356,65 @@
 
     lax.fori_loop(0, NCHUNK, project_q, 0)
 
+    def from_below(p, j):
+        if (p, j) not in up_ref:
+            return
+
+        @pl.when(up_arrives(p, j, z))
+        def _():
+            up_copy(p, j).wait_recv()
+            send_up(p, j + 1)
+            found = relay_for(p, j, 1)
+            if found:
+                @pl.when(found[1])
+                def _():
+                    relay_begin(found[0], p, up_ref[p, j], z - j)
+            spread(j, p, up_ref[p, j], z - j, True)
+
+    def from_above(p, j):
+        if (p, j) not in dn_ref:
+            return
+
+        @pl.when(dn_arrives(p, j, z))
+        def _():
+            dn_copy(p, j).wait_recv()
+            send_down(p, j + 1)
+            found = relay_for(p, j, -1)
+            if found:
+                @pl.when(found[1])
+                def _():
+                    relay_begin(found[0], p, dn_ref[p, j], z + j)
+
+            @pl.when(z + j >= NZ)
+            def _():
+                spread(HALF + j, p, dn_ref[p, j], z + j - NZ, True)
+
+    def start_second(a, p, d, source, when, second):
+        @pl.when(when)
+        def _():
+            x_copy(a, p, d, source, x, second).start()
+
+    def end_relays(wanted, rows_now):
+        for slot, p, j, dz, low, high in RELAYS:
+            if slot == wanted:
+                @pl.when((z >= low) & (z <= high) & rows_now)
+                def _():
+                    relay_end(slot, p, j, dz, z - j if dz == 1 else z + j)
+
     for j in range(1, HALF + 1):
-        for p in (K, V):
-            if (p, j) in up_ref:
-                @pl.when(up_arrives(p, j, z))
-                def _():
-                    up_copy(p, j).wait_recv()
-                    send_up(p, j + 1)
-                    found = relay_for(p, j, 1)
-                    if found:
-                        @pl.when(found[1])
-                        def _():
-                            relay_begin(found[0], p, up_ref[p, j], z - j)
-                    spread(j, p, up_ref[p, j], z - j, True)
-            if (p, j) in dn_ref:
-                @pl.when(dn_arrives(p, j, z))
-                def _():
-                    dn_copy(p, j).wait_recv()
-                    send_down(p, j + 1)
-                    found = relay_for(p, j, -1)
-                    if found:
-                        @pl.when(found[1])
-                        def _():
-                            relay_begin(found[0], p, dn_ref[p, j], z + j)
-
-                    @pl.when(z + j >= NZ)
-                    def _():
-                        spread(HALF + j, p, dn_ref[p, j], z + j - NZ, True)
-        for slot, p, rj, dz, low, high in RELAYS:
-            if rj == j:
-                @pl.when((z >= low) & (z <= high))
-                def _():
-                    relay_end(slot, p, rj, dz, z - rj if dz == 1 else z + rj)
+        if j == HALF - 1:
+            end_relays(0, z == 0)
+        if j == HALF:
+            end_relays(1, z == LAST - 1)
+        from_above(V, j)
+        if j == HALF - 1:
+            end_relays(0, z != 0)
+        if j == HALF:
+            each_x(start_second, True)
+            end_relays(1, z != LAST - 1)
+        from_below(K, j)
+        from_above(K, j)
+        from_below(V, j)
         if j == 2:
             for i in (0, 1):
                 wy(*y_recvs[i]).wait_recv()
@@ -376,29 +431,27 @@
         (0, K, HALF - 1, -1, z == LAST),
         (1, V, HALF, -1, z == LAST),
     ]
-    for slot, p, j, dz, when in divided:
+    def wait_divided(second):
+        for slot, p, j, dz, when in divided:
+            if slot == 1 or not second:
+                @pl.when(when)
+                def _():
+                    relay_z_copy(slot, p, j, dz, z - j if dz == 1 else z + j - NZ, second).wait_recv()
+
+    def wait_x(a, p, d, source, when, second):
+        sender = (x + NX - d) % NX
+
+        @pl.when(sender < x if when is None else when)
+        def _():
+            x_copy(a, p, d, source, sender, second).wait_recv()
+
+    each_x(wait_x)
+    wait_divided(False)
+
+    def place_second(a, p, d, source, when, second):
         @pl.when(when)
         def _():
-            relay_z_copy(slot, p, j, dz, z - j if dz == 1 else z + j - NZ).wait_recv()
-
-    def each_x(act):
-        for p in (K, V):
-            for d in range(1, NX):
-                act(0, p, d, z, None)
-                for j in range(1, HALF + 1):
-                    if (p, j) in up_ref:
-                        act(j, p, d, z - j, up_arrives(p, j, z))
-                    if (p, j) in dn_ref:
-                        act(HALF + j, p, d, z + j - NZ, dn_arrives(p, j, z) & (z + j >= NZ))
-
-    def wait_x(a, p, d, source, when):
-        sender = (x + NX - d) % NX
-
-        @pl.when(sender < x if when is None else when)
-        def _():
-            x_copy(a, p, d, source, sender).wait_recv()
-
-    each_x(wait_x)
+            uni[p][source * NX + (x + NX - d) % NX, FIRST:NQB] = late_x[LATE[a, p]][d - 1][...]
 
     far_count = jnp.minimum(kv, NFAR)
     near_row = lax.broadcasted_iota(jnp.int32, (2 * SPAN, SPAN), 0) & (SPAN - 1)
@@ -412,7 +465,7 @@
         )
 
     def attend_block(i, kb, vb):
-        b = (tp + 1 + i) % TP
+        b = block_at(i, 1)
         kb[0:SPAN] = own_k[pl.ds(b * (SPAN // KSPAN), SPAN // KSPAN)].reshape(SPAN, HEAD)
         vb[0:SPAN] = own_v[pl.ds(b * (SPAN // KSPAN), SPAN // KSPAN)].reshape(SPAN, HEAD)
         for j in range(NFAR):
@@ -434,7 +487,18 @@
         return jnp.concatenate([mixed[:SPAN], mixed[SPAN:]], axis=1)
 
     def attend(i, carry):
-        first, second = (tp + 1 + 2 * i) % TP, (tp + 2 + 2 * i) % TP
+        @pl.when(i == FIRST // 2)
+        def _():
+            each_x(wait_x, True)
+            wait_divided(True)
+            each_x(place_second, True)
+            for _, p, j, dz, when in divided[1::2]:
+                @pl.when(when)
+                def _():
+                    source = z - j if dz == 1 else z + j - NZ
+                    uni[p][pl.ds(source * NX, NX), FIRST:NQB] = late_relay[p][...]
+
+        first, second = block_at(2 * i, 1), block_at(2 * i + 1, 1)
         one = attend_block(2 * i, kb.at[0], vb.at[0])
         two = attend_block(2 * i + 1, kb.at[1], vb.at[1])
         att[first] = one
@@ -456,7 +520,7 @@
         return jnp.dot(piece, wfull[g], preferred_element_type=jnp.float32).astype(jnp.bfloat16).astype(jnp.float32)
 
     def gather(i, carry):
-        g, h = (tp + TP - 1 - 2 * i) % TP, (tp + TP - 2 - 2 * i) % TP
+        g, h = block_at(2 * i, -1), block_at(2 * i + 1, -1)
         att_copy(tp, g).wait_recv()
         att_copy(tp, h).wait_recv()
         acc[...] += part_of(att_all[g], g) + part_of(att_all[h], h)
@@ -464,7 +528,7 @@
 
     acc[...] = part_of(att[tp], tp)
     lax.fori_loop(0, TP // 2 - 1, gather, 0)
-    last = (tp + 1) % TP
+    last = block_at(TP - 2, -1)
     att_copy(tp, last).wait_recv()
     out_ref[...] = (acc[...] + part_of(att_all[last], last)).astype(jnp.bfloat16)
 
@@ -500,16 +564,19 @@
             for d in range(1, NX):
                 relay_x_copy(slot, d, x).wait_send()
             relay_z_copy(slot, p, rj + 1, dz, z - rj if dz == 1 else z + rj).wait_send()
-
-    def wait_sent(a, p, d, source, when):
+            if slot == 1:
+                relay_z_copy(slot, p, rj + 1, dz, z - rj if dz == 1 else z + rj, True).wait_send()
+
+    def wait_sent(a, p, d, source, when, second):
         @pl.when(x + d < NX if when is None else when)
         def _():
-            x_copy(a, p, d, source, x).wait_send()
+            x_copy(a, p, d, source, x, second).wait_send()
 
     each_x(wait_sent)
+    each_x(wait_sent, True)
 
     def att_sent(i, carry):
-        b = (tp + 1 + i) % TP
+        b = block_at(i, 1)
         att_copy(b, tp).wait_send()
         return carry
 
@@ -524,7 +591,7 @@
     arrivals = 2 * HALF + 1
     return pl.pallas_call(
         kernel,
-        out_shape=jax.ShapeDtypeStruct((SPAN, WIDTH), bf16),
+        out_shape=pltpu.VMEM((SPAN, WIDTH), bf16),
         in_specs=[any_space] * 6,
         out_specs=pl.BlockSpec(memory_space=pltpu.VMEM),
         scratch_shapes=[
@@ -544,6 +611,8 @@
             pltpu.VMEM((arrivals * 2 * (NX - 1), NQB, KSPAN, HEAD), bf16),
             [pltpu.VMEM((NX, NQB, KSPAN, HEAD), bf16) for _ in range(2)],
             pltpu.VMEM((2 * (NX - 1), NQB, KSPAN, HEAD), bf16),
+            [[pltpu.VMEM((FIRST, KSPAN, HEAD), bf16) for _ in range(NX - 1)] for _ in LATE],
+            [pltpu.VMEM((NX, FIRST, KSPAN, HEAD), bf16) for _ in range(2)],
             pltpu.VMEM((2 * NX, NQB, 128), jnp.int32),
             pltpu.SMEM((2 * NX, NQB, 128), jnp.int32),
             pltpu.VMEM((2, LISTED, HEAD), bf16),
@@ -553,7 +622,8 @@
             pltpu.VMEM((SPAN, WIDTH), jnp.float32),
             dma((NCHUNK,)), dma((3,)), dma((1,)), dma((3 * NX,)), dma((2 * NX,)), dma((2 * NX,)),
             dma((2, HALF + 1)), dma((2, HALF + 1)), dma((2, HALF + 1)), dma((2, HALF + 1)),
-            dma((arrivals, 2, NX - 1)), dma((arrivals, 2, NX - 1)), dma((2, NX)), dma((2, NX)),
+            dma((arrivals, 2, NX - 1)), dma((arrivals, 2, NX - 1)),
+            dma((len(LATE), NX - 1)), dma((len(LATE), NX - 1)), dma((2, NX)), dma((2, NX)), dma((2,)), dma((2,)),
             dma((4,)), dma((4,)), dma((5,)), dma((5,)), dma((TP,)), dma((TP,)),
         ],
         compiler_params=pltpu.CompilerParams(

time: 67.4 us -> 62.3 us (0.924)
  Pallas kernels: 65.4 us -> 61.4 us
  local copies, waits for them, and re-layouts: 1.88 us -> 0.8 us
    pallas_call x1, Pallas kernels: 65.4 us -> 61.4 us  [shards(): pl.pallas_call(kernel, out_shape=pltpu.VMEM((SPAN, WIDTH), bf16), in_spec...]
    unnamed x1, local copies, waits for them, and re-layouts: 1.88 us -> 0.8 us
where the time goes in v3:
time: 62.3 us; the launch traced here: 62.2 us
  Pallas kernels  61.4 us (99%)
  local copies, waits for them, and re-layouts  0.8 us (1%)
    pallas_call x1, Pallas kernels, shards(): pl.pallas_call(kernel, out_shape=pltpu.VMEM((SPAN, WIDTH), bf16), in_spec...  61.4 us

profile of v3, /device:TPU:193, one launch (start us, length us, event | category | flops | bytes accessed | tf_op | source)
XLA Modules:
  0.0 62.2 jit_solution(17003962578245228956)
XLA Ops:
  0.0 61.4 %sparse_attention_layer.1 = bf16[128,2048]{1,0:T(8,128)(2,1)S(1)} custom-call(bf16[1024,2048]{1,0:T(8,128)(2,1)} %tok_h.1, bf16[2048,256]{1,0:T(8,128)(2,1)} %wq_h.1, bf16[2048,128]{1,0:T(8,128)(2,1)} %wk_h.1, bf16[2048,128]{1,0:T(8,128)(2,1)} %wv_h.1, bf16[256,2048]{1,0:T(8,128)(2,1)} %wo_h.1, s32[8,12]{1,0:T(8,128)} %chosen_h.1), custom_call_target="tpu_custom_call" | custom-call | tf_op jit(solution)/shard_map/sparse_attention_layer/pallas_call | solution.py:592
  61.4 0.8 %copy.8 = bf16[128,2048]{1,0:T(8,128)(2,1)} copy(bf16[128,2048]{1,0:T(8,128)(2,1)S(1)} %sparse_attention_layer.1) | data formatting | bytes 1048576

commit v4 on v3

--- a/solution.py
+++ b/solution.py
@@ -112,6 +112,166 @@
         table = table + jnp.where((col >= 0) & ((col >> 5) == lane), col & (NBLK - 1), 0)
     tab_v[0] = table
 
+    own = {K: own_k, V: own_v}
+    up_ref = {(p, j): up_bufs[i] for i, (p, j) in enumerate(UP)}
+    dn_ref = {(p, j): dn_bufs[i] for i, (p, j) in enumerate(DOWN)}
+    uni = {K: uni_k, V: uni_v}
+
+    def z_copy(own_ref, refs, p, j, half, send, recv, step):
+        src, dst, at = own_ref if j == 1 else refs[p, j - 1], refs[p, j], j
+        if half is not None:
+            blocks = slice(half * (NBLK // 2), (half + 1) * (NBLK // 2))
+            src, dst, at = src.at[blocks], dst.at[blocks], 1 - half
+        return pltpu.make_async_remote_copy(
+            src_ref=src, dst_ref=dst, send_sem=send.at[p, at], recv_sem=recv.at[p, at],
+            device_id=at_z(step), device_id_type=MESH,
+        )
+
+    def up_copy(p, j, half=None):
+        return z_copy(own[p], up_ref, p, j, half, up_send, up_recv, 1)
+
+    def dn_copy(p, j, half=None):
+        return z_copy(own[p], dn_ref, p, j, half, dn_send, dn_recv, -1)
+
+    def halves(p, j, first):
+        return (0, 1) if (p, j) == (first, 1) else (None,)
+
+    def send_own(half):
+        @pl.when(up_arrives(K, 1, z + 1))
+        def _():
+            up_copy(K, 1, half).start()
+
+        @pl.when(dn_arrives(V, 1, (z + NZ - 1) % NZ))
+        def _():
+            dn_copy(V, 1, half).start()
+
+        if half == 1:
+            send_up(V, 1)
+            send_down(K, 1)
+
+    def up_arrives(p, j, here):
+        first = LAST if (p, j) == (V, HALF - 1) else j
+        return (here >= first) & (here <= LAST)
+
+    def dn_arrives(p, j, here):
+        source = (here + j) % NZ
+        lands = source <= (HALF - 2 if p == K else HALF - 1)
+        if (p, j) in ((K, HALF - 1), (V, HALF)):
+            lands = lands & (here != LAST)
+        return lands
+
+    def send_up(p, j):
+        if (p, j) in up_ref:
+            @pl.when(up_arrives(p, j, z + 1))
+            def _():
+                up_copy(p, j).start()
+
+    def send_down(p, j):
+        if (p, j) in dn_ref:
+            @pl.when(dn_arrives(p, j, (z + NZ - 1) % NZ))
+            def _():
+                dn_copy(p, j).start()
+
+    RELAYS = [
+        (0, V, HALF - 2, 1, HALF - 2, LAST - 2),
+        (1, K, HALF - 1, 1, HALF - 1, LAST - 1),
+        (0, K, HALF - 2, -1, 0, 0),
+        (1, V, HALF - 1, -1, 0, 0),
+    ]
+
+    def relay_x_copy(slot, d, sender_x):
+        return pltpu.make_async_remote_copy(
+            src_ref=relay_stage.at[slot * (NX - 1) + d - 1], dst_ref=relay_bufs[slot].at[sender_x],
+            send_sem=r_send.at[slot, d], recv_sem=r_recv.at[slot, d],
+            device_id=at_x(d), device_id_type=MESH,
+        )
+
+    def relay_z_copy(slot, p, j, dz, source, second=False):
+        send, recv = (up_send, up_recv) if dz == 1 else (dn_send, dn_recv)
+        send, recv = (rl_send.at[p], rl_recv.at[p]) if second else (send.at[p, j], recv.at[p, j])
+        part = slice(0, NQB) if slot == 0 else slice(FIRST, NQB) if second else slice(0, FIRST)
+        return pltpu.make_async_remote_copy(
+            src_ref=relay_bufs[slot].at[:, part],
+            dst_ref=late_relay[p] if second else uni[p].at[pl.ds(source * NX, NX), part],
+            send_sem=send, recv_sem=recv,
+            device_id=at_z(dz), device_id_type=MESH,
+        )
+
+    def relay_begin(slot, p, buf, source):
+        group = source * NX + x
+
+        def pick(i, carry):
+            b = block_at(i, 1)
+            for d in range(NX):
+                block = buf[tab_s[NX + (NX - d) % NX, b, group]]
+                if d == 0:
+                    relay_bufs[slot][x, i] = block
+                else:
+                    relay_stage[slot * (NX - 1) + d - 1, i] = block
+            return carry
+
+        lax.fori_loop(0, NQB, pick, 0)
+        for d in range(1, NX):
+            relay_x_copy(slot, d, x).start()
+
+    def relay_end(slot, p, j, dz, source):
+        for d in range(1, NX):
+            relay_x_copy(slot, d, (x + NX - d) % NX).wait_recv()
+        relay_z_copy(slot, p, j + 1, dz, source).start()
+        if slot == 1:
+            relay_z_copy(slot, p, j + 1, dz, source, True).start()
+
+    def relay_for(p, j, dz):
+        for slot, rp, rj, rdz, low, high in RELAYS:
+            if (rp, rj, rdz) == (p, j, dz):
+                return slot, (z >= low) & (z <= high)
+        return None
+
+    def stage_at(a, p, d):
+        return (a * 2 + p) * (NX - 1) + d - 1
+
+    def x_copy(a, p, d, source, sender_x, second=False):
+        late = LATE.get((a, p))
+        part = slice(0, NQB) if late is None else slice(FIRST, NQB) if second else slice(0, FIRST)
+        return pltpu.make_async_remote_copy(
+            src_ref=stage.at[stage_at(a, p, d), part],
+            dst_ref=late_x[late][d - 1] if second else uni[p].at[source * NX + sender_x, part],
+            send_sem=xl_send.at[late, d - 1] if second else x_send.at[a, p, d - 1],
+            recv_sem=xl_recv.at[late, d - 1] if second else x_recv.at[a, p, d - 1],
+            device_id=at_x(d), device_id_type=MESH,
+        )
+
+    def spread(a, p, buf, source, mine):
+        group = source * NX + x
+
+        def pick(i, carry):
+            b = block_at(i, 1)
+            for d in range(1, NX):
+                stage[stage_at(a, p, d), i] = buf[tab_s[NX - d, b, group]]
+            if mine:
+                uni[p][group, i] = buf[tab_s[0, b, group]]
+            return carry
+
+        lax.fori_loop(0, NQB, pick, 0)
+        for d in range(1, NX):
+            if mine:
+                x_copy(a, p, d, source, x).start()
+            else:
+                @pl.when(x + d < NX)
+                def _():
+                    x_copy(a, p, d, source, x).start()
+
+    def each_x(act, second=False):
+        for p in (K, V):
+            for d in range(1, NX):
+                for a, source, when in [(0, z, None)] + [
+                    (j, z - j, up_arrives(p, j, z)) for j in range(1, HALF + 1) if (p, j) in up_ref
+                ] + [
+                    (HALF + j, z + j - NZ, dn_arrives(p, j, z) & (z + j >= NZ)) for j in range(1, HALF + 1) if (p, j) in dn_ref
+                ]:
+                    if not second or (a, p) in LATE:
+                        act(a, p, d, source, when, second)
+
     w_copies[0].wait()
     w_copies[1].wait()
 
@@ -121,11 +281,16 @@
         blocks = pl.ds(i * (CHUNK // KSPAN), CHUNK // KSPAN)
         own_k[blocks] = pair[:, :HEAD].reshape(CHUNK // KSPAN, KSPAN, HEAD)
         own_v[blocks] = pair[:, HEAD:].reshape(CHUNK // KSPAN, KSPAN, HEAD)
+
+        @pl.when(i == NCHUNK // 2 - 1)
+        def _():
+            pl.semaphore_wait(bar, 2 * NX + NX - 1 + TP - 1)
+            send_own(0)
+
         return carry
 
     lax.fori_loop(0, NCHUNK, project_kv, 0)
-
-    pl.semaphore_wait(bar, 2 * NX + NX - 1 + TP - 1)
+    send_own(1)
 
     def tab_copy(d):
         return pltpu.make_async_remote_copy(
@@ -185,151 +350,6 @@
     wy(*y_sends[1]).start()
     wd(*d_sends[0]).start()
 
-    own = {K: own_k, V: own_v}
-    up_ref = {(p, j): up_bufs[i] for i, (p, j) in enumerate(UP)}
-    dn_ref = {(p, j): dn_bufs[i] for i, (p, j) in enumerate(DOWN)}
-    uni = {K: uni_k, V: uni_v}
-
-    def up_copy(p, j):
-        src = own[p] if j == 1 else up_ref[p, j - 1]
-        return pltpu.make_async_remote_copy(
-            src_ref=src, dst_ref=up_ref[p, j], send_sem=up_send.at[p, j], recv_sem=up_recv.at[p, j],
-            device_id=at_z(1), device_id_type=MESH,
-        )
-
-    def dn_copy(p, j):
-        src = own[p] if j == 1 else dn_ref[p, j - 1]
-        return pltpu.make_async_remote_copy(
-            src_ref=src, dst_ref=dn_ref[p, j], send_sem=dn_send.at[p, j], recv_sem=dn_recv.at[p, j],
-            device_id=at_z(-1), device_id_type=MESH,
-        )
-
-    def up_arrives(p, j, here):
-        first = LAST if (p, j) == (V, HALF - 1) else j
-        return (here >= first) & (here <= LAST)
-
-    def dn_arrives(p, j, here):
-        source = (here + j) % NZ
-        lands = source <= (HALF - 2 if p == K else HALF - 1)
-        if (p, j) in ((K, HALF - 1), (V, HALF)):
-            lands = lands & (here != LAST)
-        return lands
-
-    def send_up(p, j):
-        if (p, j) in up_ref:
-            @pl.when(up_arrives(p, j, z + 1))
-            def _():
-                up_copy(p, j).start()
-
-    def send_down(p, j):
-        if (p, j) in dn_ref:
-            @pl.when(dn_arrives(p, j, (z + NZ - 1) % NZ))
-            def _():
-                dn_copy(p, j).start()
-
-    RELAYS = [
-        (0, V, HALF - 2, 1, HALF - 2, LAST - 2),
-        (1, K, HALF - 1, 1, HALF - 1, LAST - 1),
-        (0, K, HALF - 2, -1, 0, 0),
-        (1, V, HALF - 1, -1, 0, 0),
-    ]
-
-    def relay_x_copy(slot, d, sender_x):
-        return pltpu.make_async_remote_copy(
-            src_ref=relay_stage.at[slot * (NX - 1) + d - 1], dst_ref=relay_bufs[slot].at[sender_x],
-            send_sem=r_send.at[slot, d], recv_sem=r_recv.at[slot, d],
-            device_id=at_x(d), device_id_type=MESH,
-        )
-
-    def relay_z_copy(slot, p, j, dz, source, second=False):
-        send, recv = (up_send, up_recv) if dz == 1 else (dn_send, dn_recv)
-        send, recv = (rl_send.at[p], rl_recv.at[p]) if second else (send.at[p, j], recv.at[p, j])
-        part = slice(0, NQB) if slot == 0 else slice(FIRST, NQB) if second else slice(0, FIRST)
-        return pltpu.make_async_remote_copy(
-            src_ref=relay_bufs[slot].at[:, part],
-            dst_ref=late_relay[p] if second else uni[p].at[pl.ds(source * NX, NX), part],
-            send_sem=send, recv_sem=recv,
-            device_id=at_z(dz), device_id_type=MESH,
-        )
-
-    def relay_begin(slot, p, buf, source):
-        group = source * NX + x
-
-        def pick(i, carry):
-            b = block_at(i, 1)
-            for d in range(NX):
-                block = buf[tab_s[NX + (NX - d) % NX, b, group]]
-                if d == 0:
-                    relay_bufs[slot][x, i] = block
-                else:
-                    relay_stage[slot * (NX - 1) + d - 1, i] = block
-            return carry
-
-        lax.fori_loop(0, NQB, pick, 0)
-        for d in range(1, NX):
-            relay_x_copy(slot, d, x).start()
-
-    def relay_end(slot, p, j, dz, source):
-        for d in range(1, NX):
-            relay_x_copy(slot, d, (x + NX - d) % NX).wait_recv()
-        relay_z_copy(slot, p, j + 1, dz, source).start()
-        if slot == 1:
-            relay_z_copy(slot, p, j + 1, dz, source, True).start()
-
-    def relay_for(p, j, dz):
-        for slot, rp, rj, rdz, low, high in RELAYS:
-            if (rp, rj, rdz) == (p, j, dz):
-                return slot, (z >= low) & (z <= high)
-        return None
-
-    def stage_at(a, p, d):
-        return (a * 2 + p) * (NX - 1) + d - 1
-
-    def x_copy(a, p, d, source, sender_x, second=False):
-        late = LATE.get((a, p))
-        part = slice(0, NQB) if late is None else slice(FIRST, NQB) if second else slice(0, FIRST)
-        return pltpu.make_async_remote_copy(
-            src_ref=stage.at[stage_at(a, p, d), part],
-            dst_ref=late_x[late][d - 1] if second else uni[p].at[source * NX + sender_x, part],
-            send_sem=xl_send.at[late, d - 1] if second else x_send.at[a, p, d - 1],
-            recv_sem=xl_recv.at[late, d - 1] if second else x_recv.at[a, p, d - 1],
-            device_id=at_x(d), device_id_type=MESH,
-        )
-
-    def spread(a, p, buf, source, mine):
-        group = source * NX + x
-
-        def pick(i, carry):
-            b = block_at(i, 1)
-            for d in range(1, NX):
-                stage[stage_at(a, p, d), i] = buf[tab_s[NX - d, b, group]]
-            if mine:
-                uni[p][group, i] = buf[tab_s[0, b, group]]
-            return carry
-
-        lax.fori_loop(0, NQB, pick, 0)
-        for d in range(1, NX):
-            if mine:
-                x_copy(a, p, d, source, x).start()
-            else:
-                @pl.when(x + d < NX)
-                def _():
-                    x_copy(a, p, d, source, x).start()
-
-    def each_x(act, second=False):
-        for p in (K, V):
-            for d in range(1, NX):
-                for a, source, when in [(0, z, None)] + [
-                    (j, z - j, up_arrives(p, j, z)) for j in range(1, HALF + 1) if (p, j) in up_ref
-                ] + [
-                    (HALF + j, z + j - NZ, dn_arrives(p, j, z) & (z + j >= NZ)) for j in range(1, HALF + 1) if (p, j) in dn_ref
-                ]:
-                    if not second or (a, p) in LATE:
-                        act(a, p, d, source, when, second)
-
-    for p in (K, V):
-        send_up(p, 1)
-        send_down(1 - p, 1)
 
     for d in range(1, NX):
         tab_copy(d).wait_recv()
@@ -362,22 +382,38 @@
 
         @pl.when(up_arrives(p, j, z))
         def _():
-            up_copy(p, j).wait_recv()
+            for half in halves(p, j, K):
+                up_copy(p, j, half).wait_recv()
             send_up(p, j + 1)
             found = relay_for(p, j, 1)
             if found:
                 @pl.when(found[1])
                 def _():
                     relay_begin(found[0], p, up_ref[p, j], z - j)
+            if (p, j) != HELD:
+                spread(j, p, up_ref[p, j], z - j, True)
+            else:
+                @pl.when(jnp.logical_not(found[1]))
+                def _():
+                    spread(j, p, up_ref[p, j], z - j, True)
+
+    HELD = (V, HALF - 2)
+
+    def spread_held():
+        p, j = HELD
+
+        @pl.when(up_arrives(p, j, z) & relay_for(p, j, 1)[1])
+        def _():
             spread(j, p, up_ref[p, j], z - j, True)
 
-    def from_above(p, j):
+    def from_above(p, j, rows_now=None):
         if (p, j) not in dn_ref:
             return
 
-        @pl.when(dn_arrives(p, j, z))
-        def _():
-            dn_copy(p, j).wait_recv()
+        @pl.when(dn_arrives(p, j, z) if rows_now is None else dn_arrives(p, j, z) & rows_now)
+        def _():
+            for half in halves(p, j, V):
+                dn_copy(p, j, half).wait_recv()
             send_down(p, j + 1)
             found = relay_for(p, j, -1)
             if found:
@@ -401,29 +437,45 @@
                 def _():
                     relay_end(slot, p, j, dz, z - j if dz == 1 else z + j)
 
-    for j in range(1, HALF + 1):
-        if j == HALF - 1:
-            end_relays(0, z == 0)
-        if j == HALF:
-            end_relays(1, z == LAST - 1)
-        from_above(V, j)
-        if j == HALF - 1:
-            end_relays(0, z != 0)
-        if j == HALF:
-            each_x(start_second, True)
-            end_relays(1, z != LAST - 1)
-        from_below(K, j)
-        from_above(K, j)
-        from_below(V, j)
-        if j == 2:
+    def weights_far(rows_now):
+        @pl.when(rows_now)
+        def _():
             for i in (0, 1):
                 wy(*y_recvs[i]).wait_recv()
                 wy(*y_sends[2 + i]).start()
                 wd(*d_sends[1 + i]).start()
-        if j == HALF:
-            for i in (2, 3):
-                wy(*y_recvs[i]).wait_recv()
-                wd(*d_sends[1 + i]).start()
+
+    fifth = z == LAST - 2
+    for j in range(1, HALF - 2):
+        from_above(V, j)
+        from_below(K, j)
+        from_above(K, j)
+        from_below(V, j)
+    j = HALF - 2
+    from_above(V, j)
+    from_below(K, j)
+    from_above(K, j)
+    from_above(V, j + 1, fifth)
+    from_below(V, j)
+    weights_far((z <= HALF) | (z == LAST))
+    j = HALF - 1
+    end_relays(0, z == 0)
+    from_above(V, j, jnp.logical_not(fifth))
+    from_above(K, j, fifth)
+    weights_far((z > HALF) & (z < LAST))
+    end_relays(0, z != 0)
+    from_below(K, j)
+    spread_held()
+    from_above(K, j, jnp.logical_not(fifth))
+    from_below(V, j)
+    j = HALF
+    end_relays(1, z == LAST - 1)
+    from_above(V, j)
+    each_x(start_second, True)
+    end_relays(1, z != LAST - 1)
+    for i in (2, 3):
+        wy(*y_recvs[i]).wait_recv()
+        wd(*d_sends[1 + i]).start()
 
     divided = [
         (0, V, HALF - 1, 1, (z >= HALF - 1) & (z <= LAST - 1)),
@@ -552,11 +604,13 @@
     for (p, j) in up_ref:
         @pl.when(up_arrives(p, j, z + 1))
         def _():
-            up_copy(p, j).wait_send()
+            for half in halves(p, j, K):
+                up_copy(p, j, half).wait_send()
     for (p, j) in dn_ref:
         @pl.when(dn_arrives(p, j, (z + NZ - 1) % NZ))
         def _():
-            dn_copy(p, j).wait_send()
+            for half in halves(p, j, V):
+                dn_copy(p, j, half).wait_send()
 
     for slot, p, rj, dz, low, high in RELAYS:
         @pl.when((z >= low) & (z <= high))

time: 62.3 us -> 60.5 us (0.971); the launches traced: 62.2 us -> 59.7 us
  Pallas kernels: 61.4 us -> 58.9 us
    pallas_call x1, Pallas kernels: 61.4 us -> 58.9 us  [shards(): pl.pallas_call(kernel, out_shape=pltpu.VMEM((SPAN, WIDTH), bf16), in_spec...]
where the time goes in v4:
time: 60.5 us; the launch traced here: 59.7 us
  Pallas kernels  58.9 us (97%)
  local copies, waits for them, and re-layouts  0.8 us (1%)
    pallas_call x1, Pallas kernels, shards(): pl.pallas_call(kernel, out_shape=pltpu.VMEM((SPAN, WIDTH), bf16), in_spec...  58.9 us

profile of v4, /device:TPU:193, one launch (start us, length us, event | category | flops | bytes accessed | tf_op | source)
XLA Modules:
  0.0 59.7 jit_solution(13178649332607535324)
XLA Ops:
  0.0 58.9 %sparse_attention_layer.1 = bf16[128,2048]{1,0:T(8,128)(2,1)S(1)} custom-call(bf16[1024,2048]{1,0:T(8,128)(2,1)} %tok_h.1, bf16[2048,256]{1,0:T(8,128)(2,1)} %wq_h.1, bf16[2048,128]{1,0:T(8,128)(2,1)} %wk_h.1, bf16[2048,128]{1,0:T(8,128)(2,1)} %wv_h.1, bf16[256,2048]{1,0:T(8,128)(2,1)} %wo_h.1, s32[8,12]{1,0:T(8,128)} %chosen_h.1), custom_call_target="tpu_custom_call" | custom-call | tf_op jit(solution)/shard_map/sparse_attention_layer/pallas_call | solution.py:646
  58.9 0.8 %copy.8 = bf16[128,2048]{1,0:T(8,128)(2,1)} copy(bf16[128,2048]{1,0:T(8,128)(2,1)S(1)} %sparse_attention_layer.1) | data formatting | bytes 1048576

commit v5 on v4

--- a/solution.py
+++ b/solution.py
@@ -22,7 +22,7 @@
 QW = 256
 GROUPS = NZ * NX
 LISTED = SPAN + NFAR * KSPAN
-CHUNK = 256
+CHUNK = 512
 NCHUNK = TOK // CHUNK
 LOG_SCALE = HEAD ** (-0.5) * 1.4426950408889634
 K, V = 0, 1
@@ -572,7 +572,7 @@
         return jnp.dot(piece, wfull[g], preferred_element_type=jnp.float32).astype(jnp.bfloat16).astype(jnp.float32)
 
     def gather(i, carry):
-        g, h = block_at(2 * i, -1), block_at(2 * i + 1, -1)
+        g, h = block_at(2 * i + 2 * (i // 2), -1), block_at(2 * i + 1 - i // 2, -1)
         att_copy(tp, g).wait_recv()
         att_copy(tp, h).wait_recv()
         acc[...] += part_of(att_all[g], g) + part_of(att_all[h], h)
@@ -580,7 +580,7 @@
 
     acc[...] = part_of(att[tp], tp)
     lax.fori_loop(0, TP // 2 - 1, gather, 0)
-    last = block_at(TP - 2, -1)
+    last = block_at(TP - 3, -1)
     att_copy(tp, last).wait_recv()
     out_ref[...] = (acc[...] + part_of(att_all[last], last)).astype(jnp.bfloat16)
 

time: 60.5 us -> 60.2 us (level)
  no operation moved by 1% of the time
where the time goes in v5:
time: 60.2 us; the launch traced here: 59.3 us
  Pallas kernels  58.5 us (97%)
  local copies, waits for them, and re-layouts  0.8 us (1%)
    pallas_call x1, Pallas kernels, shards(): pl.pallas_call(kernel, out_shape=pltpu.VMEM((SPAN, WIDTH), bf16), in_spec...  58.5 us

profile of v5, /device:TPU:193, one launch (start us, length us, event | category | flops | bytes accessed | tf_op | source)
XLA Modules:
  0.0 59.3 jit_solution(8561903655056185136)
XLA Ops:
  0.0 58.5 %sparse_attention_layer.1 = bf16[128,2048]{1,0:T(8,128)(2,1)S(1)} custom-call(bf16[1024,2048]{1,0:T(8,128)(2,1)} %tok_h.1, bf16[2048,256]{1,0:T(8,128)(2,1)} %wq_h.1, bf16[2048,128]{1,0:T(8,128)(2,1)} %wk_h.1, bf16[2048,128]{1,0:T(8,128)(2,1)} %wv_h.1, bf16[256,2048]{1,0:T(8,128)(2,1)} %wo_h.1, s32[8,12]{1,0:T(8,128)} %chosen_h.1), custom_call_target="tpu_custom_call" | custom-call | tf_op jit(solution)/shard_map/sparse_attention_layer/pallas_call | solution.py:646
  58.5 0.8 %copy.8 = bf16[128,2048]{1,0:T(8,128)(2,1)} copy(bf16[128,2048]{1,0:T(8,128)(2,1)S(1)} %sparse_attention_layer.1) | data formatting | bytes 1048576

commit v6 on v5

--- a/solution.py
+++ b/solution.py
@@ -551,11 +551,9 @@
                     uni[p][pl.ds(source * NX, NX), FIRST:NQB] = late_relay[p][...]
 
         first, second = block_at(2 * i, 1), block_at(2 * i + 1, 1)
-        one = attend_block(2 * i, kb.at[0], vb.at[0])
-        two = attend_block(2 * i + 1, kb.at[1], vb.at[1])
-        att[first] = one
-        att[second] = two
+        att[first] = attend_block(2 * i, kb.at[0], vb.at[0])
         att_copy(first, tp).start()
+        att[second] = attend_block(2 * i + 1, kb.at[1], vb.at[1])
 
         @pl.when(i < TP // 2 - 1)
         def _():

time: 60.2 us -> 60.1 us (level)
  no operation moved by 1% of the time
where the time goes in v6:
time: 60.1 us; the launch traced here: 58.9 us
  Pallas kernels  58.1 us (97%)
  local copies, waits for them, and re-layouts  0.8 us (1%)
    pallas_call x1, Pallas kernels, shards(): pl.pallas_call(kernel, out_shape=pltpu.VMEM((SPAN, WIDTH), bf16), in_spec...  58.1 us

profile of v6, /device:TPU:193, one launch (start us, length us, event | category | flops | bytes accessed | tf_op | source)
XLA Modules:
  0.0 58.9 jit_solution(15050300210227280657)
XLA Ops:
  0.0 58.1 %sparse_attention_layer.1 = bf16[128,2048]{1,0:T(8,128)(2,1)S(1)} custom-call(bf16[1024,2048]{1,0:T(8,128)(2,1)} %tok_h.1, bf16[2048,256]{1,0:T(8,128)(2,1)} %wq_h.1, bf16[2048,128]{1,0:T(8,128)(2,1)} %wk_h.1, bf16[2048,128]{1,0:T(8,128)(2,1)} %wv_h.1, bf16[256,2048]{1,0:T(8,128)(2,1)} %wo_h.1, s32[8,12]{1,0:T(8,128)} %chosen_h.1), custom_call_target="tpu_custom_call" | custom-call | tf_op jit(solution)/shard_map/sparse_attention_layer/pallas_call | solution.py:644
  58.2 0.8 %copy.8 = bf16[128,2048]{1,0:T(8,128)(2,1)} copy(bf16[128,2048]{1,0:T(8,128)(2,1)S(1)} %sparse_attention_layer.1) | data formatting | bytes 1048576
